TPU v7x, 512 devices: a whole 4x8x8 slice. The times are simulated.
512 devices in a mesh: ep: 128 (over z, y, core), tp: 4 (over x).
Axes of the slice: x: 4, y: 8, z: 8, core: 2. Of those that a mesh axis runs over, the one named last changes fastest.
Arguments:
- hidden_in: bfloat16 [2048, 1024], P('ep'), may hold values from -6 to 6
- prior_state: float32 [2048, 8, 128, 128], P('ep', 'tp'), may hold values from -4 to 4
- mix_gain: float32 [1024], replicated, may hold values from 0.1 to 1.9
- query_w: bfloat16 [1024, 1024], P(None, 'tp'), may hold values from -0.1875 to 0.1875
- key_w: bfloat16 [1024, 1024], P(None, 'tp'), may hold values from -0.1875 to 0.1875
- value_w: bfloat16 [1024, 1024], P(None, 'tp'), may hold values from -0.1875 to 0.1875
- decay_w: bfloat16 [1024, 8], P(None, 'tp'), may hold values from -0.1875 to 0.1875
- beta_w: bfloat16 [1024, 8], P(None, 'tp'), may hold values from -0.1875 to 0.1875
- decay_rate: float32 [8], P('tp'), may hold values from 0.05 to 3
- head_gain: float32 [128], replicated, may hold values from 0.1 to 1.9
- out_w: bfloat16 [1024, 1024], P('tp'), may hold values from -0.1875 to 0.1875
- ffn_gain: float32 [1024], replicated, may hold values from 0.1 to 1.9
- expert_ids: int32 [2048, 2], P('ep'), may hold values from 0 to 127, all different within a row; in each aligned block of 16 rows (0 to 15, 16 to 31, ...) at most 2 rows name the same one
- group_share: float32 [2048], P('ep'), may hold values from 0.3 to 1
- expert_share: float32 [2048, 2], P('ep'), may hold values from 0.1 to 1
- expert_gate: bfloat16 [128, 1024, 512], P('ep', None, 'tp'), may hold values from -0.1875 to 0.1875
- expert_up: bfloat16 [128, 1024, 512], P('ep', None, 'tp'), may hold values from -0.1875 to 0.1875
- expert_down: bfloat16 [128, 512, 1024], P('ep', 'tp'), may hold values from -0.25 to 0.25
- dense_gate: bfloat16 [4096, 1024], P('ep', 'tp'), may hold values from -0.1875 to 0.1875
- dense_up: bfloat16 [4096, 1024], P('ep', 'tp'), may hold values from -0.1875 to 0.1875
- dense_down: bfloat16 [4096, 1024], P('ep', 'tp'), may hold values from -0.25 to 0.25
- branch_gate: bfloat16 [1024], replicated, may hold values from -0.1875 to 0.1875
Outputs:
- layer_out: bfloat16 [2048, 1024], P('ep', 'tp')
Inputs may be any that keep to these rules, and one draw needn't show every extreme that they name: `expert_ids`: each row names 2 different experts. Among the rows of one device, no expert is named by more than 2 rows, and in every draw some expert is named by exactly 2 rows of some device.
All inputs are finite; a program needn't handle non-finite values.
Results may differ from a plain program's by a relative error of at most 0.02.
Values may be sent and summed in bfloat16 or wider, within the bound.
No kernel may reach another device: no remote copies, remote signals or barrier semaphores. Data moves between devices by JAX's collectives and lax.ppermute only.
A program may use at most 64 MiB of HBM per device.

v0:
```python
import jax
import jax.numpy as jnp
from jax import lax
from jax.sharding import Mesh
from jax.sharding import PartitionSpec as P

EP = ("ep_0", "ep_1", "ep_2")


def in_blocks(shard, dim, count):
    before, after = (shard.shape[:dim], shard.shape[dim + 1 :])
    return jnp.moveaxis(shard.reshape(*before, count, -1, *after), dim, 0)


def sum_at_owner(shard, axis, dim):
    count = lax.axis_size(axis)
    blocks = lax.all_to_all(in_blocks(shard, dim, count), axis, 0, 0, tiled=True)
    return jnp.sum(blocks.astype(jnp.float32), axis=0)


def sent_together(arrays, axis, dim, along):
    ends, at = ([], 0)
    for a in arrays[:-1]:
        at += a.shape[along]
        ends.append(at)
    both = jnp.concatenate(arrays, axis=along)
    return tuple(jnp.split(lax.all_gather(both, axis, axis=dim, tiled=True), ends, axis=along))


def sent_to_all(shard, axis):
    copies = jnp.broadcast_to(shard, (lax.axis_size(axis), *shard.shape))
    return lax.all_to_all(copies, axis, split_axis=0, concat_axis=0, tiled=True)


def over_copies(shard, axis):
    everything = sent_to_all(shard, axis)
    return jnp.sum(everything.astype(jnp.float32), axis=0)


def in_order(blocks, dim):
    blocks = jnp.moveaxis(blocks, 0, dim)
    shape = blocks.shape
    return blocks.reshape(*shape[:dim], shape[dim] * shape[dim + 1], *shape[dim + 2 :])


def gather_axes(shard, axes, dim):
    far, near = axes
    initial = sent_to_all(shard, far)
    blocks = jnp.swapaxes(sent_to_all(initial, near), 0, 1)
    return in_order(blocks.reshape(-1, *shard.shape), dim)


def sum_by_axis(shard, axes, dim):
    far, near = axes
    blocks = in_blocks(shard, dim, lax.axis_size(far))
    nearer = sum_at_owner(blocks, near, dim + 1)
    arrived = lax.all_to_all(
        nearer.astype(jnp.bfloat16), far, split_axis=0, concat_axis=0, tiled=True
    )
    return arrived.astype(jnp.float32).sum(axis=0)


def rms_scale(values, gain, floor):
    return values * lax.rsqrt(jnp.mean(values * values, axis=-1, keepdims=True) + floor) * gain


def unit_rows(values):
    return values * lax.rsqrt(jnp.sum(values * values, axis=-1, keepdims=True) + 1.0)


def delta_read(queries, key_rows, value_rows, beta_vals, decay_vals, prior_state):
    stacked = jnp.stack([queries, key_rows], axis=2)
    readout = jnp.einsum("shcd,shde->shce", stacked, prior_state, precision=lax.Precision.HIGHEST)
    intersection = jnp.sum(queries * key_rows, axis=-1) * beta_vals
    return decay_vals[..., None] * readout[:, :, 0] + intersection[..., None] * (
        value_rows - decay_vals[..., None] * readout[:, :, 1]
    )


def expert_rows(row_block, w_gate, w_up, w_down):
    gate_pre = jnp.dot(row_block, w_gate, preferred_element_type=jnp.float32)
    up_pre = jnp.dot(row_block, w_up, preferred_element_type=jnp.float32)
    hidden = (jax.nn.silu(gate_pre) * up_pre).astype(jnp.bfloat16)
    partial_out = jnp.dot(hidden, w_down, preferred_element_type=jnp.float32)
    return sum_at_owner(partial_out.astype(jnp.bfloat16), "tp", 1)


def branch_terms(row_block, w_gate, w_up):
    contract = (((1,), (1,)), ((), ()))
    gate_pre = lax.dot_general(w_gate, row_block, contract, preferred_element_type=jnp.float32)
    up_pre = lax.dot_general(w_up, row_block, contract, preferred_element_type=jnp.float32)
    return jnp.stack([gate_pre, up_pre])


def whole_hidden(row_block, w_gate, w_up):
    terms = branch_terms(row_block, w_gate, w_up)
    return (jax.nn.silu(terms[0]) * terms[1]).astype(jnp.bfloat16)


def branch_project(hidden_cols, w_down):
    return lax.dot_general(
        hidden_cols, w_down, (((0,), (0,)), ((), ())), preferred_element_type=jnp.float32
    )


def local(
    hidden_in,
    prior_state,
    mix_gain,
    query_w,
    key_w,
    value_w,
    decay_w,
    beta_w,
    decay_rate,
    head_gain,
    out_w,
    ffn_gain,
    expert_ids,
    group_share,
    expert_share,
    expert_gate,
    expert_up,
    expert_down,
    dense_gate,
    dense_up,
    dense_down,
    branch_gate,
):
    seq_dev, model_width = hidden_in.shape
    heads_local = prior_state.shape[1]
    key_size = prior_state.shape[2]
    value_size = prior_state.shape[3]
    topk_count = expert_ids.shape[1]
    n_ep = lax.axis_size(EP)
    quarter = model_width // lax.axis_size("tp")
    offset = lax.axis_index("tp") * quarter
    capacity = min(seq_dev, 2 * seq_dev * topk_count // n_ep + 2)
    slot_total = n_ep * capacity
    gate_whole, up_whole = sent_together((dense_gate, dense_up), "tp", 1, 0)
    normed = rms_scale(hidden_in.astype(jnp.float32), mix_gain, 0.1).astype(jnp.bfloat16)
    queries = unit_rows(
        jnp.dot(normed, query_w, preferred_element_type=jnp.float32).reshape(
            seq_dev, heads_local, key_size
        )
    )
    key_rows = unit_rows(
        jnp.dot(normed, key_w, preferred_element_type=jnp.float32).reshape(
            seq_dev, heads_local, key_size
        )
    )
    value_rows = jnp.dot(normed, value_w, preferred_element_type=jnp.float32).reshape(
        seq_dev, heads_local, value_size
    )
    beta_vals = jax.nn.sigmoid(jnp.dot(normed, beta_w, preferred_element_type=jnp.float32))
    decay_vals = jnp.exp(
        -decay_rate * jax.nn.softplus(jnp.dot(normed, decay_w, preferred_element_type=jnp.float32))
    )
    readout = delta_read(queries, key_rows, value_rows, beta_vals, decay_vals, prior_state)
    head_out = (
        rms_scale(readout, head_gain, 0.01)
        .astype(jnp.bfloat16)
        .reshape(seq_dev, heads_local * value_size)
    )
    partial_out = jnp.dot(head_out, out_w, preferred_element_type=jnp.float32).astype(jnp.bfloat16)
    mix = over_copies(partial_out, "tp").astype(jnp.float32)
    resid = (hidden_in.astype(jnp.float32) + mix).astype(jnp.bfloat16)
    normed2 = rms_scale(resid.astype(jnp.float32), ffn_gain, 0.1).astype(jnp.bfloat16)
    resid_own = lax.dynamic_slice_in_dim(resid, offset, quarter, 1).astype(jnp.float32)
    route_weight = (
        group_share[:, None] * expert_share / jnp.sum(expert_share, axis=1, keepdims=True)
    )
    rows_all = lax.all_gather(normed2, EP, axis=0, tiled=True)
    ids_all, weight_all = (
        gather_axes(expert_ids, (("ep_0", "ep_1"), "ep_2"), 0),
        gather_axes(route_weight, (("ep_0", "ep_1"), "ep_2"), 0),
    )
    total_rows = rows_all.shape[0]
    own_index = lax.axis_index(EP)
    matches = ids_all == own_index
    token_weight = jnp.sum(jnp.where(matches, weight_all, 0.0), axis=1)
    routed = jnp.any(matches, axis=1)
    slot_rank = jnp.cumsum(routed.astype(jnp.int32)) - 1
    target = jnp.where(routed, slot_rank, slot_total)
    source = (
        jnp.zeros((slot_total + 1,), jnp.int32)
        .at[target]
        .set(jnp.arange(total_rows, dtype=jnp.int32))[:slot_total]
    )
    is_valid = jnp.arange(slot_total) < jnp.sum(routed.astype(jnp.int32))
    summed = expert_rows(rows_all[source], expert_gate[0], expert_up[0], expert_down[0])
    expert_out = lax.optimization_barrier(summed.astype(jnp.bfloat16)).astype(jnp.float32)
    row_scale = jnp.where(is_valid, token_weight[source], 0.0)
    contrib = (
        jnp.zeros((total_rows, quarter), jnp.float32)
        .at[source]
        .add(expert_out * row_scale[:, None])
    )
    hidden = whole_hidden(rows_all, gate_whole, up_whole)
    branch_part = branch_project(hidden, dense_down)
    weight_rows = jax.nn.sigmoid(jnp.dot(rows_all, branch_gate, preferred_element_type=jnp.float32))
    together = sum_by_axis(
        (contrib + weight_rows[:, None] * branch_part).astype(jnp.bfloat16),
        (("ep_0", "ep_1"), "ep_2"),
        0,
    )
    result = resid_own + together
    return result.astype(jnp.bfloat16)


def solution(mesh):
    torus = Mesh(mesh.devices.reshape(8, 8, 2, mesh.shape["tp"]), ("ep_0", "ep_1", "ep_2", "tp"))
    placed = (
        P(EP, None),
        P(EP, "tp", None, None),
        P(),
        P(None, "tp"),
        P(None, "tp"),
        P(None, "tp"),
        P(None, "tp"),
        P(None, "tp"),
        P("tp"),
        P(),
        P("tp", None),
        P(),
        P(EP, None),
        P(EP),
        P(EP, None),
        P(EP, None, "tp"),
        P(EP, None, "tp"),
        P(EP, "tp", None),
        P(EP, "tp"),
        P(EP, "tp"),
        P(EP, "tp"),
        P(),
    )
    return jax.shard_map(local, mesh=torus, in_specs=placed, out_specs=P(EP, "tp"), check_vma=False)
```

profile of v0, /device:TPU:1, one launch (start us, length us, event | category | flops | bytes accessed | tf_op | source)
XLA Modules:
  0.0 183.0 jit_solution(2401194961620052772)
XLA Ops:
  6.5 1.0 fusion.29
  7.6 1.3 fusion.60
  9.0 1.3 fusion.62
  10.4 1.3 fusion.57
  11.9 0.2 multiply_reduce_fusion.1
  12.1 0.1 broadcast_multiply_fusion
  12.3 1.9 %fusion.38 = f32[16,2,2,128]{3,2,1,0:T(2,128)S(1)} fusion(f32[16,2,128,128]{3,2,1,0:T(8,128)S(1)} %copy-done, f32[16,2,1,128]{3,2,1,0:T(1,128)S(1)} %get-tuple-element.12, f32[16,2,1,128]{3,2,1,0:T(1,128)S(1)} %get-tuple-element.13), kind=kOutput, calls=%fused_computation.56 | convolution fusion | flops 12591104 | bytes 2162688 | tf_op jit(solution)/shard_map/shcd,shde->shce/dot_general | solution.py:73
  14.4 0.2 fusion.5
  14.7 0.2 fusion.51
  15.0 0.2 multiply_reduce_fusion
  15.5 0.2 convolution_convert_fusion.1
  15.7 9.5 %all_to_all.40 = bf16[4,16,1024]{2,1,0:T(8,128)(2,1)S(1)} all-to-all(bf16[4,16,1024]{2,1,0:T(8,128)(2,1)S(1)} %broadcast_in_dim.25), channel_id=1, replica_groups=mesh['ep_0'=8,'ep_1'=8,'ep_2'=2,'tp'=4] {'tp'}, dimensions={0} | all-to-all | bytes 262144 | tf_op jit(solution)/shard_map/all_to_all | solution.py:32
  25.1 0.1 fusion.26
  25.3 0.7 fusion.28
  26.0 0.7 broadcast_in_dim.32
  26.7 16.3 %all-to-all-start.4 = ((f32[64,16,2]{1,2,0:T(2,128)}), f32[64,16,2]{1,2,0:T(2,128)S(1)}, u32[]{:S(2)}, u32[]{:S(2)}) async-start(f32[64,16,2]{1,2,0:T(2,128)} %broadcast_in_dim.32), calls=%async_computation.4 | async-start | bytes 131072 | tf_op jit(solution)/shard_map/all_to_all | solution.py:32
  43.0 11.1 %all-to-all-done.4 = f32[64,16,2]{1,2,0:T(2,128)S(1)} async-done(((f32[64,16,2]{1,2,0:T(2,128)}), f32[64,16,2]{1,2,0:T(2,128)S(1)}, u32[]{:S(2)}, u32[]{:S(2)}) %all-to-all-start.4) | async-done | bytes 8224 | tf_op jit(solution)/shard_map/all_to_all | solution.py:32
  54.3 6.9 %all_to_all.41 = f32[2,1,2048]{2,1,0:T(1,128)S(1)} all-to-all(f32[2,1,2048]{2,1,0:T(1,128)S(1)} %reshape.215), channel_id=1, replica_groups=mesh['ep_0'=8,'ep_1'=8,'ep_2'=2,'tp'=4] {'ep_2'}, dimensions={0} | all-to-all | bytes 32768 | tf_op jit(solution)/shard_map/all_to_all | solution.py:32
  61.2 0.7 broadcast_in_dim.27
  61.9 4.6 %all-to-all-start.1 = ((s32[64,16,2]{1,2,0:T(2,128)}), s32[64,16,2]{1,2,0:T(2,128)S(1)}, u32[]{:S(2)}, u32[]{:S(2)}) async-start(s32[64,16,2]{1,2,0:T(2,128)} %broadcast_in_dim.27), calls=%async_computation.1 | async-start | bytes 131072 | tf_op jit(solution)/shard_map/all_to_all | solution.py:32
  66.5 10.0 %all_gather.7 = bf16[64,1024]{1,0:T(8,128)(2,1)S(1)} all-gather(bf16[64,256]{1,0:T(8,128)(2,1)S(1)} %pad_maximum_fusion), channel_id=1, replica_groups=mesh['ep_0'=8,'ep_1'=8,'ep_2'=2,'tp'=4] {'tp'}, dimensions={1}, use_global_device_ids=true | all-gather | bytes 163840 | tf_op jit(solution)/shard_map/all_gather | solution.py:27
  76.5 0.5 broadcast.177
  77.0 0.7 reduce.11
  78.0 5.7 %all_to_all.42 = s32[2,1,2048]{2,1,0:T(1,128)S(1)} all-to-all(s32[2,1,2048]{2,1,0:T(1,128)S(1)} %reshape.213), channel_id=1, replica_groups=mesh['ep_0'=8,'ep_1'=8,'ep_2'=2,'tp'=4] {'ep_2'}, dimensions={0} | all-to-all | bytes 32768 | tf_op jit(solution)/shard_map/all_to_all | solution.py:32
  83.7 0.5 broadcast.178
  84.2 0.7 reduce.12
  85.5 0.3 reduce-window.9
  86.0 0.1 reduce_sum.136
  86.3 8.0 %scatter_custom_fusion = s32[257]{0:T(512)S(1)} fusion(s32[2048]{0:T(1024)S(1)} %bitcast.111, s32[2048]{0:T(1024)S(1)} %iota.8, s32[]{:T(128)} %constant.18.clone.1), kind=kCustom, calls=%fused_computation.95 | custom fusion | bytes 1032 | tf_op jit(solution)/shard_map/scatter | solution.py:188
  94.4 1.7 gather_fusion.1
  96.1 0.6 convert_reduce_fusion.2
  96.8 0.6 compare_select_fusion.3
  97.4 17.9 %all-gather.2.cloned.1.call-done = bf16[2048,1024]{1,0:T(8,128)(2,1)} async-done(((bf16[16,1024]{1,0:T(8,128)(2,1)}), bf16[2048,1024]{1,0:T(8,128)(2,1)}) %all-gather.2.cloned.1.call-update) | async-done | bytes 4194320 | tf_op jit(solution)/shard_map/all_gather | solution.py:173
  115.3 4.3 %gather_fusion = bf16[256,1024]{1,0:T(8,128)(2,1)S(1)} fusion(bf16[2048,1024]{1,0:T(8,128)(2,1)} %all-gather.2.cloned.1.call-done, s32[1024]{0:T(1024)S(1)} %pad_clamp_fusion), kind=kCustom, calls=%fused_computation | custom fusion | bytes 1049600 | tf_op jit(solution)/shard_map/gather | solution.py:191
  119.6 0.3 fusion.9
  119.9 1.5 convolution_convert_fusion
  121.5 0.8 copy.121
  122.3 3.9 %all-to-all-start.3 = ((bf16[4,256,256]{2,1,0:T(8,128)(2,1)}), bf16[4,256,256]{2,1,0:T(8,128)(2,1)S(1)}, u32[]{:S(2)}, u32[]{:S(2)}) async-start(bf16[4,256,256]{2,1,0:T(8,128)(2,1)} %bitcast.96), calls=%async_computation.3 | async-start | bytes 1048576 | tf_op jit(solution)/shard_map/all_to_all | solution.py:17
  126.2 3.5 %fusion.69 = f32[1,2048]{1,0:T(1,128)S(1)} fusion(bf16[2048,1024]{1,0:T(8,128)(2,1)} %all-gather.2.cloned.1.call-done, bf16[1024,1]{0,1:T(2,128)(2,1)S(1)} %reshape.199), kind=kOutput, calls=%fused_computation.110 | convolution fusion | flops 4194304 | bytes 4204544 | tf_op jit(solution)/shard_map/dot_general | solution.py:201
  129.7 1.3 fusion.35
  131.1 5.2 %convolution_multiply_fusion = f32[2048,256]{1,0:T(8,128)} fusion(bf16[32,256]{1,0:T(8,128)(2,1)S(1)} %copy-done.6, bf16[2048,1024]{1,0:T(8,128)(2,1)} %all-gather.2.cloned.1.call-done, f32[2048]{0:T(1024)S(1)} %add_divide_fusion, f32[32,2048]{1,0:T(8,128)S(1)} %fusion.35, bf16[64,1024]{1,0:T(8,128)(2,1)S(1)} %all_gather.7), kind=kOutput, calls=%fused_computation.4 | convolution fusion | flops 168689664 | bytes 6643712 | tf_op jit(solution)/shard_map/dot_general | solution.py:101
  136.4 5.3 %scatter_custom_fusion.1 = f32[2048,256]{1,0:T(8,128)} fusion(f32[2048,256]{1,0:T(8,128)} %convolution_multiply_fusion, s32[256]{0:T(256)S(1)} %compare_select_fusion.1, bf16[256,256]{1,0:T(8,128)(2,1)S(1)} %reduce_sum.132, f32[256]{0:T(256)S(1)} %compare_select_fusion.3), kind=kCustom, calls=%fused_computation.23 | custom fusion | flops 196608 | bytes 2229248 | tf_op jit(solution)/shard_map/scatter-add | solution.py:197
  141.6 1.7 convert_element_type.81
  143.4 4.8 %all_to_all.43 = bf16[2,64,16,256]{3,2,1,0:T(8,128)(2,1)S(1)} all-to-all(bf16[2,64,16,256]{3,2,1,0:T(8,128)(2,1)S(1)} %bitcast.98), channel_id=1, replica_groups=mesh['ep_0'=8,'ep_1'=8,'ep_2'=2,'tp'=4] {'ep_2'}, dimensions={0} | all-to-all | bytes 2097152 | tf_op jit(solution)/shard_map/all_to_all | solution.py:17
  148.2 1.1 reduce_sum.137
  149.3 8.5 %all-to-all-start.7 = ((bf16[64,16,256]{2,1,0:T(8,128)(2,1)}), bf16[64,16,256]{2,1,0:T(8,128)(2,1)S(1)}, u32[]{:S(2)}, u32[]{:S(2)}) async-start(bf16[64,16,256]{2,1,0:T(8,128)(2,1)} %reduce_sum.137), calls=%async_computation.7 | async-start | bytes 1048576 | tf_op jit(solution)/shard_map/all_to_all | solution.py:57
  157.8 17.6 %all-to-all-done.7 = bf16[64,16,256]{2,1,0:T(8,128)(2,1)S(1)} async-done(((bf16[64,16,256]{2,1,0:T(8,128)(2,1)}), bf16[64,16,256]{2,1,0:T(8,128)(2,1)S(1)}, u32[]{:S(2)}, u32[]{:S(2)}) %all-to-all-start.7) | async-done | bytes 524320 | tf_op jit(solution)/shard_map/all_to_all | solution.py:57
  175.5 0.6 add_convert_fusion
  (95 shorter events, 2.8 us)
Async XLA Ops:
  6.5 5.7 %copy-start = (f32[16,2,128,128]{3,2,1,0:T(8,128)S(1)}, f32[16,2,128,128]{3,2,1,0:T(8,128)}, u32[]{:S(2)}) copy-start(f32[16,2,128,128]{3,2,1,0:T(8,128)} %param.23) | copy-start | bytes 6291460
  6.5 108.8 %all-gather.2.cloned.1.call-start = ((), (), s32[]{:S(2)}) async-start(), calls=%async_computation.8 | async-start | bytes 4227072 | tf_op jit(solution)/shard_map/all_gather | solution.py:173
  7.6 6.8 %copy-start.2 = (bf16[16,1024]{1,0:T(8,128)(2,1)S(1)}, bf16[16,1024]{1,0:T(8,128)(2,1)}, u32[]{:S(2)}) copy-start(bf16[16,1024]{1,0:T(8,128)(2,1)} %param.22) | copy-start | bytes 98308
  7.6 6.8 %copy-start.5 = (f32[1024]{0:T(1024)S(1)}, f32[1024]{0:T(1024)}, u32[]{:S(2)}) copy-start(f32[1024]{0:T(1024)} %param.24) | copy-start | bytes 12292
  7.6 6.8 %copy-start.14 = (bf16[1024,2]{0,1:T(2,128)(2,1)S(1)}, bf16[1024,2]{0,1:T(2,128)(2,1)}, u32[]{:S(2)}) copy-start(bf16[1024,2]{0,1:T(2,128)(2,1)} %param.29) | copy-start | bytes 12292
  8.9 5.7 %copy-start.16 = (f32[2]{0:T(128)S(1)}, f32[2]{0:T(128)}, u32[]{:S(2)}) copy-start(f32[2]{0:T(128)} %param.30) | copy-start | bytes 28
  8.9 5.7 %copy-start.15 = (bf16[1024,2]{0,1:T(2,128)(2,1)S(1)}, bf16[1024,2]{0,1:T(2,128)(2,1)}, u32[]{:S(2)}) copy-start(bf16[1024,2]{0,1:T(2,128)(2,1)} %param.28) | copy-start | bytes 12292
  8.9 6.3 %copy-start.17 = (f32[128]{0:T(128)S(1)}, f32[128]{0:T(128)}, u32[]{:S(2)}) copy-start(f32[128]{0:T(128)} %param.31) | copy-start | bytes 1540
  9.0 6.5 %copy-start.3 = (bf16[256,1024]{1,0:T(8,128)(2,1)S(1)}, bf16[256,1024]{1,0:T(8,128)(2,1)}, u32[]{:S(2)}) copy-start(bf16[256,1024]{1,0:T(8,128)(2,1)} %param.32) | copy-start | bytes 1572868
  12.1 13.2 %copy-start.9 = (f32[1024]{0:T(1024)S(1)}, f32[1024]{0:T(1024)}, u32[]{:S(2)}) copy-start(f32[1024]{0:T(1024)} %param.33) | copy-start | bytes 12292
  12.3 13.7 %copy-start.10 = (f32[16,2]{0,1:T(2,128)S(1)}, f32[16,2]{0,1:T(2,128)}, u32[]{:S(2)}) copy-start(f32[16,2]{0,1:T(2,128)} %param.36) | copy-start | bytes 388
  12.3 13.7 %copy-start.13 = (f32[16]{0:T(128)S(1)}, f32[16]{0:T(128)}, u32[]{:S(2)}) copy-start(f32[16]{0:T(128)} %param.35) | copy-start | bytes 196
  12.3 30.7 %copy-start.7 = (bf16[32,256]{1,0:T(8,128)(2,1)S(1)}, bf16[32,256]{1,0:T(8,128)(2,1)}, u32[]{:S(2)}) copy-start(bf16[32,256]{1,0:T(8,128)(2,1)} %param.41) | copy-start | bytes 49156
  12.3 30.7 %copy-start.8 = (bf16[32,256]{1,0:T(8,128)(2,1)S(1)}, bf16[32,256]{1,0:T(8,128)(2,1)}, u32[]{:S(2)}) copy-start(bf16[32,256]{1,0:T(8,128)(2,1)} %param.40) | copy-start | bytes 49156
  12.3 48.9 %copy-start.12 = (s32[16,2]{0,1:T(2,128)S(1)}, s32[16,2]{0,1:T(2,128)}, u32[]{:S(2)}) copy-start(s32[16,2]{0,1:T(2,128)} %param.34) | copy-start | bytes 388
  12.3 64.1 %copy-start.11 = (bf16[1024]{0:T(1024)(128)(2,1)S(1)}, bf16[1024]{0:T(1024)(128)(2,1)}, u32[]{:S(2)}) copy-start(bf16[1024]{0:T(1024)(128)(2,1)} %param.43) | copy-start | bytes 6148
  26.7 27.4 %all-to-all-start.4 = ((f32[64,16,2]{1,2,0:T(2,128)}), f32[64,16,2]{1,2,0:T(2,128)S(1)}, u32[]{:S(2)}, u32[]{:S(2)}) async-start(f32[64,16,2]{1,2,0:T(2,128)} %broadcast_in_dim.32), calls=%async_computation.4 | async-start | bytes 131072 | tf_op jit(solution)/shard_map/all_to_all | solution.py:32
  61.9 15.9 %all-to-all-start.1 = ((s32[64,16,2]{1,2,0:T(2,128)}), s32[64,16,2]{1,2,0:T(2,128)S(1)}, u32[]{:S(2)}, u32[]{:S(2)}) async-start(s32[64,16,2]{1,2,0:T(2,128)} %broadcast_in_dim.27), calls=%async_computation.1 | async-start | bytes 131072 | tf_op jit(solution)/shard_map/all_to_all | solution.py:32
  97.4 22.2 %copy-start.4 = (bf16[1,1024,128]{2,1,0:T(8,128)(2,1)S(1)}, bf16[1,1024,128]{2,1,0:T(8,128)(2,1)}, u32[]{:S(2)}) copy-start(bf16[1,1024,128]{2,1,0:T(8,128)(2,1)} %param.37) | copy-start | bytes 786436
  122.3 14.0 %all-to-all-start.3 = ((bf16[4,256,256]{2,1,0:T(8,128)(2,1)}), bf16[4,256,256]{2,1,0:T(8,128)(2,1)S(1)}, u32[]{:S(2)}, u32[]{:S(2)}) async-start(bf16[4,256,256]{2,1,0:T(8,128)(2,1)} %bitcast.96), calls=%async_computation.3 | async-start | bytes 1048576 | tf_op jit(solution)/shard_map/all_to_all | solution.py:17
  126.2 3.5 %copy-start.1 = (bf16[2048,1024]{1,0:T(8,128)(2,1)S(1)}, bf16[2048,1024]{1,0:T(8,128)(2,1)}, u32[]{:S(2)}) copy-start(bf16[2048,1024]{1,0:T(8,128)(2,1)} %all-gather.2.cloned.1.call-done) | copy-start | bytes 12582916
  129.7 1.4 copy-start.6
  149.3 26.1 %all-to-all-start.7 = ((bf16[64,16,256]{2,1,0:T(8,128)(2,1)}), bf16[64,16,256]{2,1,0:T(8,128)(2,1)S(1)}, u32[]{:S(2)}, u32[]{:S(2)}) async-start(bf16[64,16,256]{2,1,0:T(8,128)(2,1)} %reduce_sum.137), calls=%async_computation.7 | async-start | bytes 1048576 | tf_op jit(solution)/shard_map/all_to_all | solution.py:57
Sparse Core Ops, SparseCore 0:
  26.1 89.1 all-gather.1
where the time goes:
time: 186 us; the launch traced here: 183 us
  waiting for transfers between devices  46.6 us (25%)
  blocking collectives  36.9 us (20%)
  starting transfers between devices  33.3 us (18%)
  local copies, waits for them, and re-layouts  19.5 us (10%)
  matrix products  18.3 us (10%)
  other arithmetic  14.6 us (8%)
  between operations  13.9 us (7%)
    all_to_all x3, blocking collectives, sent_to_all(): return lax.all_to_all(copies, axis, split_axis=0, concat_axis=0, tiled=True)  22.1 us
    all_to_all x2, starting transfers between devices, sent_to_all(): return lax.all_to_all(copies, axis, split_axis=0, concat_axis=0, tiled=True)  20.9 us
    all_gather x1, waiting for transfers between devices, local(): rows_all = lax.all_gather(normed2, EP, axis=0, tiled=True)  17.9 us
    all_to_all x1, waiting for transfers between devices, sum_by_axis(): lax.all_to_all(nearer.astype(jnp.bfloat16), far, split_axis=0, concat_axi...  17.6 us
    all_to_all x2, waiting for transfers between devices, sent_to_all(): return lax.all_to_all(copies, axis, split_axis=0, concat_axis=0, tiled=True)  11.1 us
    all_gather x1, blocking collectives, sent_together(): lax.all_gather(both, axis, axis=dim, tiled=True)  9.99 us
    all_to_all x1, starting transfers between devices, sum_by_axis(): lax.all_to_all(nearer.astype(jnp.bfloat16), far, split_axis=0, concat_axi...  8.52 us
    scatter x1, local copies, waits for them, and re-layouts, local(): source = jnp.zeros((slot_total + 1,), jnp.int32).at[target].set(jnp.arang...  8.04 us
  transfers between devices with their start and end apart: 5, of which 3 were waited for; matrix products, arithmetic and copies ran while one was open for 15% of the time, Pallas kernels for 0%

commit v1 on v0

v1 whole, which is shorter than its diff:
```python
import jax
import jax.numpy as jnp
from jax import lax
from jax.sharding import Mesh
from jax.sharding import PartitionSpec as P

EP = ("z", "y", "c")
BF = jnp.bfloat16
F32 = jnp.float32


def rms_scale(values, gain, floor):
    return values * lax.rsqrt(jnp.mean(values * values, axis=-1, keepdims=True) + floor) * gain


def unit_rows(values):
    return values * lax.rsqrt(jnp.sum(values * values, axis=-1, keepdims=True) + 1.0)


def delta_read(queries, key_rows, value_rows, beta_vals, decay_vals, prior_state):
    stacked = jnp.stack([queries, key_rows], axis=2)
    readout = jnp.einsum("shcd,shde->shce", stacked, prior_state, precision=lax.Precision.HIGHEST)
    intersection = jnp.sum(queries * key_rows, axis=-1) * beta_vals
    return decay_vals[..., None] * readout[:, :, 0] + intersection[..., None] * (
        value_rows - decay_vals[..., None] * readout[:, :, 1]
    )


def dot32(a, b):
    return jnp.dot(a, b, preferred_element_type=F32)


def exchange(blocks, axis):
    return lax.all_to_all(blocks, axis, split_axis=0, concat_axis=0, tiled=True)


def local(
    hidden_in,
    prior_state,
    mix_gain,
    query_w,
    key_w,
    value_w,
    decay_w,
    beta_w,
    decay_rate,
    head_gain,
    out_w,
    ffn_gain,
    expert_ids,
    group_share,
    expert_share,
    expert_gate,
    expert_up,
    expert_down,
    dense_gate,
    dense_up,
    dense_down,
    branch_gate,
):
    rows, width = hidden_in.shape
    heads, dk, dv = prior_state.shape[1:]
    n_ep = lax.axis_size(EP)
    n_tp = lax.axis_size("x")
    n_z = lax.axis_size("z")
    quarter = width // n_tp
    cap = 2
    per_z = rows // n_z
    tp_at = lax.axis_index("x")
    hid = dense_gate.shape[0]

    dense_all = jnp.concatenate([dense_gate, dense_up, dense_down], axis=0)
    copies = jnp.broadcast_to(dense_all, (n_z, *dense_all.shape))
    dense_z = exchange(copies, "z").reshape(n_z, 3, hid, quarter)

    normed = rms_scale(hidden_in.astype(F32), mix_gain, 0.1).astype(BF)
    queries = unit_rows(dot32(normed, query_w).reshape(rows, heads, dk))
    key_rows = unit_rows(dot32(normed, key_w).reshape(rows, heads, dk))
    value_rows = dot32(normed, value_w).reshape(rows, heads, dv)
    beta_vals = jax.nn.sigmoid(dot32(normed, beta_w))
    decay_vals = jnp.exp(-decay_rate * jax.nn.softplus(dot32(normed, decay_w)))
    readout = delta_read(queries, key_rows, value_rows, beta_vals, decay_vals, prior_state)
    head_out = rms_scale(readout, head_gain, 0.01).astype(BF).reshape(rows, heads * dv)
    partial_out = dot32(head_out, out_w).astype(BF)
    partials = exchange(jnp.broadcast_to(partial_out, (n_tp, rows, width)), "x")
    mix = jnp.sum(partials.astype(F32), axis=0)
    resid = (hidden_in.astype(F32) + mix).astype(BF)
    normed2 = rms_scale(resid.astype(F32), ffn_gain, 0.1).astype(BF)
    own = lax.dynamic_slice_in_dim(normed2, tp_at * quarter, quarter, 1)
    resid_own = lax.dynamic_slice_in_dim(resid, tp_at * quarter, quarter, 1).astype(F32)
    branch_weight = jax.nn.sigmoid(dot32(normed2, branch_gate))
    route_weight = (
        group_share[:, None] * expert_share / jnp.sum(expert_share, axis=1, keepdims=True)
    )

    same = expert_ids[:, :, None, None] == expert_ids[None, None, :, :]
    earlier = jnp.arange(rows)[:, None] > jnp.arange(rows)[None, :]
    rank = jnp.sum(same & earlier[:, None, :, None], axis=(2, 3)).astype(jnp.int32)
    dest = jnp.arange(n_ep)[:, None, None, None]
    slot = jnp.arange(cap)[None, :, None, None]
    chosen = (expert_ids[None, None] == dest) & (rank[None, None] == slot)
    pick_expert = jnp.any(chosen, axis=3)
    dense_row = (jnp.arange(n_ep) // (n_ep // n_z))[:, None] * per_z + jnp.arange(per_z)[None, :]
    pick_dense = dense_row[:, :, None] == jnp.arange(rows)
    pick = jnp.concatenate([pick_expert, pick_dense], axis=1).astype(BF)
    block = cap + per_z
    sent = dot32(pick.reshape(n_ep * block, rows), own).astype(BF)
    arrived = exchange(sent.reshape(n_ep, block, quarter), EP)
    moe_rows = arrived[:, :cap].reshape(n_ep * cap, quarter)
    dense_rows = arrived[:, cap:].reshape(n_ep * per_z, quarter)

    n_hid = n_z * hid
    gate_z = dense_z[:, 0].reshape(n_hid, quarter)
    up_z = dense_z[:, 1].reshape(n_hid, quarter)
    down_z = dense_z[:, 2].reshape(n_hid, quarter)
    contract = (((1,), (1,)), ((), ()))
    gate_part = lax.dot_general(dense_rows, gate_z, contract, preferred_element_type=F32)
    up_part = lax.dot_general(dense_rows, up_z, contract, preferred_element_type=F32)
    share = n_hid // n_tp
    pre = jnp.stack(
        [gate_part.reshape(-1, n_tp, share), up_part.reshape(-1, n_tp, share)], axis=2
    ).astype(BF)
    pre = jnp.moveaxis(pre, 1, 0).reshape(n_tp, -1, 2 * share)
    moe_copies = jnp.broadcast_to(moe_rows, (n_tp, *moe_rows.shape))
    first = exchange(jnp.concatenate([moe_copies, pre], axis=2), "x")

    full_rows = jnp.moveaxis(first[:, :, :quarter], 0, 1).reshape(n_ep * cap, width)
    pre_sum = jnp.sum(first[:, :, quarter:].astype(F32), axis=0)
    dense_hidden = (jax.nn.silu(pre_sum[:, :share]) * pre_sum[:, share:]).astype(BF)
    gate_pre = dot32(full_rows, expert_gate[0])
    up_pre = dot32(full_rows, expert_up[0])
    hidden = (jax.nn.silu(gate_pre) * up_pre).astype(BF)
    expert_part = dot32(hidden, expert_down[0]).astype(BF)
    part_blocks = jnp.moveaxis(expert_part.reshape(n_ep * cap, n_tp, quarter), 1, 0)
    hidden_copies = jnp.broadcast_to(dense_hidden, (n_tp, *dense_hidden.shape))
    second = exchange(jnp.concatenate([part_blocks, hidden_copies], axis=2), "x")

    expert_out = jnp.sum(second[:, :, :quarter].astype(F32), axis=0).astype(BF)
    all_hidden = jnp.moveaxis(second[:, :, quarter:], 0, 1).reshape(n_ep * per_z, n_hid)
    dense_out = dot32(all_hidden, down_z).astype(BF)
    back = jnp.concatenate(
        [expert_out.reshape(n_ep, cap, quarter), dense_out.reshape(n_ep, per_z, quarter)], axis=1
    )
    returned = exchange(back, EP)

    slots = returned[:, :cap].reshape(n_ep * cap, quarter)
    position = expert_ids * cap + rank
    fetch = (position[:, :, None] == jnp.arange(n_ep * cap)).astype(BF)
    per_choice = dot32(fetch.reshape(rows * 2, n_ep * cap), slots).reshape(rows, 2, quarter)
    moe = jnp.sum(per_choice * route_weight[:, :, None], axis=1)
    branch = jnp.sum(
        returned[:, cap:].astype(F32).reshape(n_z, n_ep // n_z, per_z, quarter), axis=1
    ).reshape(rows, quarter)
    return (resid_own + moe + branch_weight[:, None] * branch).astype(BF)


def solution(mesh):
    torus = Mesh(mesh.devices.reshape(8, 8, 2, mesh.shape["tp"]), ("z", "y", "c", "x"))
    placed = (
        P(EP, None),
        P(EP, "x", None, None),
        P(),
        P(None, "x"),
        P(None, "x"),
        P(None, "x"),
        P(None, "x"),
        P(None, "x"),
        P("x"),
        P(),
        P("x", None),
        P(),
        P(EP, None),
        P(EP),
        P(EP, None),
        P(EP, None, "x"),
        P(EP, None, "x"),
        P(EP, "x", None),
        P(EP, "x"),
        P(EP, "x"),
        P(EP, "x"),
        P(),
    )
    return jax.shard_map(local, mesh=torus, in_specs=placed, out_specs=P(EP, "x"), check_vma=False)
```

time: 186 us -> 131 us (0.70); the launches traced: 183 us -> 130 us
  local copies, waits for them, and re-layouts: 19.5 us -> 4.85 us
  between operations: 13.9 us -> 0.56 us
  blocking collectives: 36.9 us -> 26.2 us
  other arithmetic: 14.6 us -> 5.13 us
  matrix products: 18.3 us -> 9.13 us
  waiting for transfers between devices: 46.6 us -> 49.2 us
    all_to_all x4, waiting for transfers between devices: 28.7 us -> 49.2 us  [exchange(): return lax.all_to_all(blocks, axis, split_axis=0, concat_axis=0, tiled=True)]
    all_gather x1 -> x0, waiting for transfers between devices: 17.9 us -> none  [local(): rows_all = lax.all_gather(normed2, EP, axis=0, tiled=True)]
    all_gather x1 -> x0, blocking collectives: 9.99 us -> none  [sent_together(): lax.all_gather(both, axis, axis=dim, tiled=True)]
    dot_general x11 -> x14, matrix products: 16.4 us -> 7.27 us  [the longest x12 6.84 us: dot32(): return jnp.dot(a, b, preferred_element_type=F32)]
    scatter x1 -> x0, local copies, waits for them, and re-layouts: 8.04 us -> none  [local(): source = jnp.zeros((slot_total + 1,), jnp.int32).at[target].set(jnp.arang...]
    gather x2 -> x0, local copies, waits for them, and re-layouts: 6 us -> none  [the longest x1 4.28 us: local(): rows_all[source]]
    scatter-add x1 -> x0, other arithmetic: 5.28 us -> none  [local(): contrib = jnp.zeros((total_rows, quarter), jnp.float32).at[source].add(ex...]
    convert_element_type x4 -> x3, other arithmetic: 2.98 us -> 0.8 us  [the longest x1 0.69 us: local(): return (resid_own + moe + branch_weight[:, None] * branch).astype(BF)]
  transfers between devices with their start and end apart: 5 -> 4, of which waited for: 3 -> 4; matrix products, arithmetic and copies ran while one was open for 15% -> 1% of each run, Pallas kernels for 0% -> 0%
where the time goes in v1:
time: 131 us; the launch traced here: 130 us
  waiting for transfers between devices  49.2 us (38%)
  starting transfers between devices  34.9 us (27%)
  blocking collectives  26.2 us (20%)
  matrix products  9.13 us (7%)
  other arithmetic  5.13 us (4%)
  local copies, waits for them, and re-layouts  4.85 us (4%)
    all_to_all x4, waiting for transfers between devices, exchange(): return lax.all_to_all(blocks, axis, split_axis=0, concat_axis=0, tiled=True)  49.2 us
    all_to_all x4, starting transfers between devices, exchange(): return lax.all_to_all(blocks, axis, split_axis=0, concat_axis=0, tiled=True)  34.9 us
    all_to_all x2, blocking collectives, exchange(): return lax.all_to_all(blocks, axis, split_axis=0, concat_axis=0, tiled=True)  26.2 us
    dot_general x12, matrix products, dot32(): return jnp.dot(a, b, preferred_element_type=F32)  6.84 us
  transfers between devices with their start and end apart: 4, of which 4 were waited for; matrix products, arithmetic and copies ran while one was open for 1% of the time, Pallas kernels for 0%

profile of v1, /device:TPU:1, one launch (start us, length us, event | category | flops | bytes accessed | tf_op | source)
XLA Modules:
  0.0 130.0 jit_solution(16190794996811055197)
XLA Ops:
  0.0 1.0 fusion.25
  1.1 1.3 fusion.57
  2.4 1.3 fusion.55
  3.7 0.7 neg.21
  4.4 0.7 broadcast_bitcast_fusion
  5.1 1.0 fusion.47
  6.1 0.1 multiply_reduce_fusion.3
  6.3 0.1 multiply_reduce_fusion.2
  6.4 0.2 multiply_reduce_fusion.1
  6.6 0.2 fusion.7
  6.8 0.1 copy.104
  6.9 0.2 fusion.52
  7.2 0.1 broadcast_multiply_fusion
  7.4 1.9 %fusion.31 = f32[16,2,2,128]{3,2,1,0:T(2,128)S(1)} fusion(f32[16,2,128,128]{3,2,1,0:T(8,128)S(1)} %copy-done, f32[16,2,1,128]{3,2,1,0:T(1,128)S(1)} %get-tuple-element.15, f32[16,2,1,128]{3,2,1,0:T(1,128)S(1)} %get-tuple-element.16), kind=kOutput, calls=%fused_computation.55 | convolution fusion | flops 12591104 | bytes 2162688 | tf_op jit(solution)/shard_map/shcd,shde->shce/dot_general | solution.py:22
  9.3 0.2 multiply_reduce_fusion
  9.8 0.2 convolution_convert_fusion.5
  10.0 0.7 broadcast_in_dim.8
  10.6 4.8 %all-to-all-start = ((bf16[4,16,1024]{2,1,0:T(8,128)(2,1)}), bf16[4,16,1024]{2,1,0:T(8,128)(2,1)S(1)}, u32[]{:S(2)}, u32[]{:S(2)}) async-start(bf16[4,16,1024]{2,1,0:T(8,128)(2,1)} %broadcast_in_dim.8), calls=%async_computation | async-start | bytes 262144 | tf_op jit(solution)/shard_map/all_to_all | solution.py:34
  15.6 0.2 convert_reduce_fusion.3
  15.9 0.2 copy.105
  16.0 4.2 %all-to-all-done = bf16[4,16,1024]{2,1,0:T(8,128)(2,1)S(1)} async-done(((bf16[4,16,1024]{2,1,0:T(8,128)(2,1)}), bf16[4,16,1024]{2,1,0:T(8,128)(2,1)S(1)}, u32[]{:S(2)}, u32[]{:S(2)}) %all-to-all-start) | async-done | bytes 131104 | tf_op jit(solution)/shard_map/all_to_all | solution.py:34
  20.3 0.1 fusion.22
  20.5 0.2 convolution_convert_fusion.1
  20.7 0.8 reshape.243
  21.5 19.0 %all-to-all-start.1 = ((bf16[128,4,256]{2,1,0:T(4,128)(2,1)}), bf16[128,4,256]{2,1,0:T(4,128)(2,1)S(1)}, u32[]{:S(2)}, u32[]{:S(2)}) async-start(bf16[128,4,256]{2,1,0:T(4,128)(2,1)} %reshape.243), calls=%async_computation.1 | async-start | bytes 524288 | tf_op jit(solution)/shard_map/all_to_all | solution.py:34
  40.6 15.2 %all-to-all-done.1 = bf16[128,4,256]{2,1,0:T(4,128)(2,1)S(1)} async-done(((bf16[128,4,256]{2,1,0:T(4,128)(2,1)}), bf16[128,4,256]{2,1,0:T(4,128)(2,1)S(1)}, u32[]{:S(2)}, u32[]{:S(2)}) %all-to-all-start.1) | async-done | bytes 262176 | tf_op jit(solution)/shard_map/all_to_all | solution.py:34
  55.8 0.8 broadcast_in_dim.10
  56.5 3.5 %all-to-all-start.2 = ((bf16[8,96,256]{2,1,0:T(8,128)(2,1)}), bf16[8,96,256]{2,1,0:T(8,128)(2,1)S(1)}, u32[]{:S(2)}, u32[]{:S(2)}) async-start(bf16[8,96,256]{2,1,0:T(8,128)(2,1)} %broadcast_in_dim.10), calls=%async_computation.2 | async-start | bytes 786432 | tf_op jit(solution)/shard_map/all_to_all | solution.py:34
  60.0 0.2 fusion.65
  60.2 0.1 copy.106
  60.4 14.7 %all-to-all-done.2 = bf16[8,96,256]{2,1,0:T(8,128)(2,1)S(1)} async-done(((bf16[8,96,256]{2,1,0:T(8,128)(2,1)}), bf16[8,96,256]{2,1,0:T(8,128)(2,1)S(1)}, u32[]{:S(2)}, u32[]{:S(2)}) %all-to-all-start.2) | async-done | bytes 393248 | tf_op jit(solution)/shard_map/all_to_all | solution.py:34
  75.1 0.2 fusion.1
  75.3 0.2 fusion
  75.7 14.4 %all_to_all.30 = bf16[4,256,384]{1,2,0:T(8,128)(2,1)S(1)} all-to-all(bf16[4,256,384]{1,2,0:T(8,128)(2,1)S(1)} %pad_maximum_fusion), channel_id=1, replica_groups=mesh['z'=8,'y'=8,'c'=2,'x'=4] {'x'}, dimensions={0} | all-to-all | bytes 1572864 | tf_op jit(solution)/shard_map/all_to_all | solution.py:34
  90.3 0.3 fusion.15
  90.6 1.6 %convolution_convert_fusion = bf16[256,1024]{1,0:T(8,128)(2,1)S(1)} fusion(bf16[256,1024]{0,1:T(8,128)(2,1)S(1)} %bitcast.111, bf16[1,128,1024]{2,1,0:T(8,128)(2,1)} %param.39, bf16[1,1024,128]{2,1,0:T(8,128)(2,1)} %param.38, f32[256,128]{1,0:T(8,128)S(1)} %fusion.15), kind=kOutput, calls=%fused_computation | convolution fusion | flops 134676480 | bytes 1703936 | tf_op jit(solution)/shard_map/dot_general | solution.py:30
  92.2 0.2 copy.110
  92.5 11.8 %all_to_all.31 = bf16[4,256,320]{1,2,0:T(8,128)(2,1)S(1)} all-to-all(bf16[4,256,320]{1,2,0:T(8,128)(2,1)S(1)} %pad_maximum_fusion.1), channel_id=1, replica_groups=mesh['z'=8,'y'=8,'c'=2,'x'=4] {'x'}, dimensions={0} | all-to-all | bytes 1310720 | tf_op jit(solution)/shard_map/all_to_all | solution.py:34
  104.3 0.1 copy.109
  104.5 0.2 convolution_convert_fusion.2
  104.8 1.0 pad_maximum_fusion.2
  105.8 7.7 %all-to-all-start.5 = ((bf16[128,4,256]{2,1,0:T(4,128)(2,1)}), bf16[128,4,256]{2,1,0:T(4,128)(2,1)S(1)}, u32[]{:S(2)}, u32[]{:S(2)}) async-start(bf16[128,4,256]{2,1,0:T(4,128)(2,1)} %pad_maximum_fusion.2), calls=%async_computation.5 | async-start | bytes 524288 | tf_op jit(solution)/shard_map/all_to_all | solution.py:34
  113.5 0.1 fusion.11
  113.7 15.1 %all-to-all-done.5 = bf16[128,4,256]{2,1,0:T(4,128)(2,1)S(1)} async-done(((bf16[128,4,256]{2,1,0:T(4,128)(2,1)}), bf16[128,4,256]{2,1,0:T(4,128)(2,1)S(1)}, u32[]{:S(2)}, u32[]{:S(2)}) %all-to-all-start.5) | async-done | bytes 262176 | tf_op jit(solution)/shard_map/all_to_all | solution.py:34
  128.8 0.1 slice.73
  129.0 0.2 convert_reduce_fusion.1
  129.2 0.2 fusion.3
  129.3 0.7 add_convert_fusion
  (79 shorter events, 1.7 us)
Async XLA Ops:
  0.0 7.3 %copy-start = (f32[16,2,128,128]{3,2,1,0:T(8,128)S(1)}, f32[16,2,128,128]{3,2,1,0:T(8,128)}, u32[]{:S(2)}) copy-start(f32[16,2,128,128]{3,2,1,0:T(8,128)} %param.23) | copy-start | bytes 6291460
  0.0 6.6 %copy-start.1 = (bf16[16,1024]{1,0:T(8,128)(2,1)S(1)}, bf16[16,1024]{1,0:T(8,128)(2,1)}, u32[]{:S(2)}) copy-start(bf16[16,1024]{1,0:T(8,128)(2,1)} %param.22) | copy-start | bytes 98308
  0.0 6.6 %copy-start.5 = (f32[1024]{0:T(1024)S(1)}, f32[1024]{0:T(1024)}, u32[]{:S(2)}) copy-start(f32[1024]{0:T(1024)} %param.24) | copy-start | bytes 12292
  0.0 6.6 %copy-start.14 = (bf16[1024,2]{0,1:T(2,128)(2,1)S(1)}, bf16[1024,2]{0,1:T(2,128)(2,1)}, u32[]{:S(2)}) copy-start(bf16[1024,2]{0,1:T(2,128)(2,1)} %param.29) | copy-start | bytes 12292
  0.0 6.9 %copy-start.3 = (bf16[1024,256]{1,0:T(8,128)(2,1)S(1)}, bf16[1024,256]{1,0:T(8,128)(2,1)}, u32[]{:S(2)}) copy-start(bf16[1024,256]{1,0:T(8,128)(2,1)} %param.27) | copy-start | bytes 1572868
  6.8 2.9 %copy-start.2 = (bf16[256,1024]{1,0:T(8,128)(2,1)S(1)}, bf16[256,1024]{1,0:T(8,128)(2,1)}, u32[]{:S(2)}) copy-start(bf16[256,1024]{1,0:T(8,128)(2,1)} %param.32) | copy-start | bytes 1572868
  7.3 8.2 %copy-start.6 = (s32[16,2]{0,1:T(2,128)S(1)}, s32[16,2]{0,1:T(2,128)}, u32[]{:S(2)}) copy-start(s32[16,2]{0,1:T(2,128)} %param.34) | copy-start | bytes 388
  7.3 13.1 %copy-start.10 = (f32[1024]{0:T(1024)S(1)}, f32[1024]{0:T(1024)}, u32[]{:S(2)}) copy-start(f32[1024]{0:T(1024)} %param.33) | copy-start | bytes 12292
  9.5 31.1 %copy-start.7 = (bf16[32,256]{1,0:T(8,128)(2,1)S(1)}, bf16[32,256]{1,0:T(8,128)(2,1)}, u32[]{:S(2)}) copy-start(bf16[32,256]{1,0:T(8,128)(2,1)} %param.42) | copy-start | bytes 49156
  9.5 31.1 %copy-start.8 = (bf16[32,256]{1,0:T(8,128)(2,1)S(1)}, bf16[32,256]{1,0:T(8,128)(2,1)}, u32[]{:S(2)}) copy-start(bf16[32,256]{1,0:T(8,128)(2,1)} %param.41) | copy-start | bytes 49156
  9.5 31.0 %copy-start.9 = (bf16[32,256]{1,0:T(8,128)(2,1)S(1)}, bf16[32,256]{1,0:T(8,128)(2,1)}, u32[]{:S(2)}) copy-start(bf16[32,256]{1,0:T(8,128)(2,1)} %param.40) | copy-start | bytes 49156
  10.6 9.7 %all-to-all-start = ((bf16[4,16,1024]{2,1,0:T(8,128)(2,1)}), bf16[4,16,1024]{2,1,0:T(8,128)(2,1)S(1)}, u32[]{:S(2)}, u32[]{:S(2)}) async-start(bf16[4,16,1024]{2,1,0:T(8,128)(2,1)} %broadcast_in_dim.8), calls=%async_computation | async-start | bytes 262144 | tf_op jit(solution)/shard_map/all_to_all | solution.py:34
  21.5 34.3 %all-to-all-start.1 = ((bf16[128,4,256]{2,1,0:T(4,128)(2,1)}), bf16[128,4,256]{2,1,0:T(4,128)(2,1)S(1)}, u32[]{:S(2)}, u32[]{:S(2)}) async-start(bf16[128,4,256]{2,1,0:T(4,128)(2,1)} %reshape.243), calls=%async_computation.1 | async-start | bytes 524288 | tf_op jit(solution)/shard_map/all_to_all | solution.py:34
  56.5 18.5 %all-to-all-start.2 = ((bf16[8,96,256]{2,1,0:T(8,128)(2,1)}), bf16[8,96,256]{2,1,0:T(8,128)(2,1)S(1)}, u32[]{:S(2)}, u32[]{:S(2)}) async-start(bf16[8,96,256]{2,1,0:T(8,128)(2,1)} %broadcast_in_dim.10), calls=%async_computation.2 | async-start | bytes 786432 | tf_op jit(solution)/shard_map/all_to_all | solution.py:34
  75.7 14.6 %copy-start.4 = (bf16[1,1024,128]{2,1,0:T(8,128)(2,1)S(1)}, bf16[1,1024,128]{2,1,0:T(8,128)(2,1)}, u32[]{:S(2)}) copy-start(bf16[1,1024,128]{2,1,0:T(8,128)(2,1)} %param.37) | copy-start | bytes 786436
  104.3 9.2 %copy-start.12 = (bf16[1024]{0:T(1024)(128)(2,1)S(1)}, bf16[1024]{0:T(1024)(128)(2,1)}, u32[]{:S(2)}) copy-start(bf16[1024]{0:T(1024)(128)(2,1)} %param.43) | copy-start | bytes 6148
  104.3 9.2 %copy-start.11 = (f32[16,2]{0,1:T(2,128)S(1)}, f32[16,2]{0,1:T(2,128)}, u32[]{:S(2)}) copy-start(f32[16,2]{0,1:T(2,128)} %param.36) | copy-start | bytes 388
  104.3 9.3 %copy-start.13 = (f32[16]{0:T(128)S(1)}, f32[16]{0:T(128)}, u32[]{:S(2)}) copy-start(f32[16]{0:T(128)} %param.35) | copy-start | bytes 196
  105.8 23.0 %all-to-all-start.5 = ((bf16[128,4,256]{2,1,0:T(4,128)(2,1)}), bf16[128,4,256]{2,1,0:T(4,128)(2,1)S(1)}, u32[]{:S(2)}, u32[]{:S(2)}) async-start(bf16[128,4,256]{2,1,0:T(4,128)(2,1)} %pad_maximum_fusion.2), calls=%async_computation.5 | async-start | bytes 524288 | tf_op jit(solution)/shard_map/all_to_all | solution.py:34

commit v2 on v1

--- a/solution.py
+++ b/solution.py
@@ -1,6 +1,8 @@
 import jax
 import jax.numpy as jnp
 from jax import lax
+from jax.experimental import pallas as pl
+from jax.experimental.pallas import tpu as pltpu
 from jax.sharding import Mesh
 from jax.sharding import PartitionSpec as P
 
@@ -17,17 +19,88 @@
     return values * lax.rsqrt(jnp.sum(values * values, axis=-1, keepdims=True) + 1.0)
 
 
-def delta_read(queries, key_rows, value_rows, beta_vals, decay_vals, prior_state):
-    stacked = jnp.stack([queries, key_rows], axis=2)
-    readout = jnp.einsum("shcd,shde->shce", stacked, prior_state, precision=lax.Precision.HIGHEST)
-    intersection = jnp.sum(queries * key_rows, axis=-1) * beta_vals
-    return decay_vals[..., None] * readout[:, :, 0] + intersection[..., None] * (
-        value_rows - decay_vals[..., None] * readout[:, :, 1]
-    )
-
-
 def dot32(a, b):
     return jnp.dot(a, b, preferred_element_type=F32)
+
+
+def mixer_body(
+    hidden_ref,
+    state_ref,
+    gain_ref,
+    query_ref,
+    key_ref,
+    value_ref,
+    decay_ref,
+    beta_ref,
+    rate_ref,
+    head_gain_ref,
+    out_w_ref,
+    partial_ref,
+    read_q,
+    read_k,
+):
+    rows, heads, dk, dv = state_ref.shape
+    wide = hidden_ref[...].astype(F32)
+    normed = rms_scale(wide, gain_ref[...], 0.1).astype(BF)
+    wide = normed.astype(F32)
+    q_all = dot32(normed, query_ref[...])
+    k_all = dot32(normed, key_ref[...])
+    units = []
+    for source in (q_all, k_all):
+        for h in range(heads):
+            units.append(unit_rows(source[:, h * dk : (h + 1) * dk]))
+    used = 2 * heads * rows
+    stacked = jnp.concatenate(units + [jnp.zeros((dk - used, dk), F32)], axis=0)
+    columns = stacked.T
+    for h in range(heads):
+        for s in range(rows):
+            state = state_ref[s, h]
+            q_col = columns[:, h * rows + s : h * rows + s + 1]
+            k_at = (heads + h) * rows + s
+            k_col = columns[:, k_at : k_at + 1]
+            lanes = slice(h * dv, (h + 1) * dv)
+            read_q[s : s + 1, lanes] = jnp.sum(state * q_col, axis=0, keepdims=True)
+            read_k[s : s + 1, lanes] = jnp.sum(state * k_col, axis=0, keepdims=True)
+    v_all = dot32(normed, value_ref[...])
+    outs = []
+    for h in range(heads):
+        lanes = slice(h * dv, (h + 1) * dv)
+        decay_in = jnp.sum(wide * decay_ref[h : h + 1, :].astype(F32), axis=1, keepdims=True)
+        beta_in = jnp.sum(wide * beta_ref[h : h + 1, :].astype(F32), axis=1, keepdims=True)
+        decay = jnp.exp(-rate_ref[h] * jax.nn.softplus(decay_in))
+        meet = jnp.sum(units[h] * units[heads + h], axis=1, keepdims=True)
+        meet = meet * jax.nn.sigmoid(beta_in)
+        readout = decay * read_q[:, lanes] + meet * (v_all[:, lanes] - decay * read_k[:, lanes])
+        outs.append(rms_scale(readout, head_gain_ref[...], 0.01).astype(BF))
+    head_out = jnp.concatenate(outs, axis=1)
+    partial_ref[...] = dot32(head_out, out_w_ref[...]).astype(BF)
+
+
+def mixer(hidden, state, gain, query, key, value, decay, beta, rate, head_gain, out_w):
+    rows, width = hidden.shape
+    vmem = pl.BlockSpec(memory_space=pltpu.VMEM)
+    smem = pl.BlockSpec(memory_space=pltpu.SMEM)
+    wide = state.shape[1] * state.shape[3]
+    return pl.pallas_call(
+        mixer_body,
+        out_shape=jax.ShapeDtypeStruct((rows, width), BF),
+        in_specs=[vmem] * 8 + [smem] + [vmem] * 2,
+        out_specs=vmem,
+        scratch_shapes=[pltpu.VMEM((rows, wide), F32), pltpu.VMEM((rows, wide), F32)],
+        name="mixer",
+    )(
+        hidden,
+        state,
+        gain[None],
+        query,
+        key,
+        value,
+        decay.T,
+        beta.T,
+        rate,
+        head_gain[None],
+        out_w,
+    )
 
 
 def exchange(blocks, axis):
@@ -59,7 +132,6 @@
     branch_gate,
 ):
     rows, width = hidden_in.shape
-    heads, dk, dv = prior_state.shape[1:]
     n_ep = lax.axis_size(EP)
     n_tp = lax.axis_size("x")
     n_z = lax.axis_size("z")
@@ -73,16 +145,20 @@
     copies = jnp.broadcast_to(dense_all, (n_z, *dense_all.shape))
     dense_z = exchange(copies, "z").reshape(n_z, 3, hid, quarter)
 
-    normed = rms_scale(hidden_in.astype(F32), mix_gain, 0.1).astype(BF)
-    queries = unit_rows(dot32(normed, query_w).reshape(rows, heads, dk))
-    key_rows = unit_rows(dot32(normed, key_w).reshape(rows, heads, dk))
-    value_rows = dot32(normed, value_w).reshape(rows, heads, dv)
-    beta_vals = jax.nn.sigmoid(dot32(normed, beta_w))
-    decay_vals = jnp.exp(-decay_rate * jax.nn.softplus(dot32(normed, decay_w)))
-    readout = delta_read(queries, key_rows, value_rows, beta_vals, decay_vals, prior_state)
-    head_out = rms_scale(readout, head_gain, 0.01).astype(BF).reshape(rows, heads * dv)
-    partial_out = dot32(head_out, out_w).astype(BF)
-    partials = exchange(jnp.broadcast_to(partial_out, (n_tp, rows, width)), "x")
+    partial_out = mixer(
+        hidden_in,
+        prior_state,
+        mix_gain,
+        query_w,
+        key_w,
+        value_w,
+        decay_w,
+        beta_w,
+        decay_rate,
+        head_gain,
+        out_w,
+    )
+    partials = lax.all_gather(partial_out, "x")
     mix = jnp.sum(partials.astype(F32), axis=0)
     resid = (hidden_in.astype(F32) + mix).astype(BF)
     normed2 = rms_scale(resid.astype(F32), ffn_gain, 0.1).astype(BF)

time: 131 us -> 129 us (0.985)
  blocking collectives: 26.2 us -> 36.7 us
  matrix products: 9.13 us -> 2.06 us
  Pallas kernels: 0 us -> 5.19 us
  waiting for transfers between devices: 49.2 us -> 45 us
  starting transfers between devices: 34.9 us -> 31.9 us
  local copies, waits for them, and re-layouts: 4.85 us -> 3.33 us
    all_gather x0 -> x1, blocking collectives: none -> 10.6 us  [local(): partials = lax.all_gather(partial_out, 'x')]
    dot_general x12 -> x6, matrix products: 6.84 us -> 1.63 us  [dot32(): return jnp.dot(a, b, preferred_element_type=F32)]
    pallas_call x0 -> x1, Pallas kernels: none -> 5.19 us  [mixer(): pl.pallas_call(mixer_body, out_shape=jax.ShapeDtypeStruct((rows, width),...]
    all_to_all x4 -> x3, waiting for transfers between devices: 49.2 us -> 45 us  [exchange(): return lax.all_to_all(blocks, axis, split_axis=0, concat_axis=0, tiled=True)]
    all_to_all x4 -> x3, starting transfers between devices: 34.9 us -> 31.9 us  [exchange(): return lax.all_to_all(blocks, axis, split_axis=0, concat_axis=0, tiled=True)]
    dot_general x1 -> x0, matrix products: 1.86 us -> none  [delta_read(): jnp.einsum('shcd,shde->shce', stacked, prior_state, precision=lax.Precisi...]
  transfers between devices with their start and end apart: 4 -> 3, of which waited for: 4 -> 3; matrix products, arithmetic and copies ran while one was open for 1% -> 0% of each run, Pallas kernels for 0% -> 0%
where the time goes in v2:
time: 129 us
  waiting for transfers between devices  45 us (35%)
  blocking collectives  36.7 us (28%)
  starting transfers between devices  31.9 us (25%)
  Pallas kernels  5.19 us (4%)
  other arithmetic  4.21 us (3%)
  local copies, waits for them, and re-layouts  3.33 us (3%)
  matrix products  2.06 us (2%)
    all_to_all x3, waiting for transfers between devices, exchange(): return lax.all_to_all(blocks, axis, split_axis=0, concat_axis=0, tiled=True)  45 us
    all_to_all x3, starting transfers between devices, exchange(): return lax.all_to_all(blocks, axis, split_axis=0, concat_axis=0, tiled=True)  31.9 us
    all_to_all x2, blocking collectives, exchange(): return lax.all_to_all(blocks, axis, split_axis=0, concat_axis=0, tiled=True)  26.1 us
    all_gather x1, blocking collectives, local(): partials = lax.all_gather(partial_out, 'x')  10.6 us
    pallas_call x1, Pallas kernels, mixer(): pl.pallas_call(mixer_body, out_shape=jax.ShapeDtypeStruct((rows, width),...  5.19 us
  transfers between devices with their start and end apart: 3, of which 3 were waited for; matrix products, arithmetic and copies ran while one was open for 0% of the time, Pallas kernels for 0%

profile of v2, /device:TPU:1, one launch (start us, length us, event | category | flops | bytes accessed | tf_op | source)
XLA Modules:
  0.0 128.8 jit_solution(5736634296565011169)
XLA Ops:
  0.0 0.8 iota_compare_fusion.2
  0.8 0.9 convert_reduce_fusion.3
  1.8 0.1 and_reduce_fusion
  1.9 0.2 copy.51
  2.1 0.0 copy-start.3
  2.1 0.0 copy-start.8
  2.1 5.2 %mixer.1 = bf16[16,1024]{1,0:T(8,128)(2,1)} custom-call(bf16[16,1024]{1,0:T(8,128)(2,1)} %hidden_ref.1, f32[16,2,128,128]{3,2,1,0:T(8,128)} %state_ref.1, f32[1,1024]{1,0:T(1,128)} %bitcast.76, bf16[1024,256]{1,0:T(8,128)(2,1)} %query_ref.1, bf16[1024,256]{1,0:T(8,128)(2,1)} %key_ref.1, bf16[1024,256]{1,0:T(8,128)(2,1)} %value_ref.1, ...), custom_call_target="tpu_custom_call" | custom-call | tf_op jit(solution)/shard_map/mixer/pallas_call | solution.py:84
  7.3 10.6 %all-gather = bf16[64,1024]{1,0:T(8,128)(2,1)S(1)} all-gather(bf16[16,1024]{1,0:T(8,128)(2,1)} %mixer.1), channel_id=2, replica_groups=mesh['z'=8,'y'=8,'c'=2,'x'=4] {'x'}, dimensions={0}, use_global_device_ids=true | all-gather | bytes 163840 | tf_op jit(solution)/shard_map/all_gather | solution.py:161
  17.9 0.1 fusion.18
  18.1 0.0 copy-done.8
  18.1 0.1 fusion.20
  18.2 0.2 convolution_convert_fusion.1
  18.4 0.8 reshape.164
  19.1 20.5 %all-to-all-start = ((bf16[128,4,256]{2,1,0:T(4,128)(2,1)}), bf16[128,4,256]{2,1,0:T(4,128)(2,1)S(1)}, u32[]{:S(2)}, u32[]{:S(2)}) async-start(bf16[128,4,256]{2,1,0:T(4,128)(2,1)} %reshape.164), calls=%async_computation | async-start | bytes 524288 | tf_op jit(solution)/shard_map/all_to_all | solution.py:107
  39.6 0.0 copy-done.5
  39.6 0.0 copy-done.6
  39.7 15.2 %all-to-all-done = bf16[128,4,256]{2,1,0:T(4,128)(2,1)S(1)} async-done(((bf16[128,4,256]{2,1,0:T(4,128)(2,1)}), bf16[128,4,256]{2,1,0:T(4,128)(2,1)S(1)}, u32[]{:S(2)}, u32[]{:S(2)}) %all-to-all-start) | async-done | bytes 262176 | tf_op jit(solution)/shard_map/all_to_all | solution.py:107
  54.9 0.8 broadcast_in_dim.13
  55.6 3.5 %all-to-all-start.1 = ((bf16[8,96,256]{2,1,0:T(8,128)(2,1)}), bf16[8,96,256]{2,1,0:T(8,128)(2,1)S(1)}, u32[]{:S(2)}, u32[]{:S(2)}) async-start(bf16[8,96,256]{2,1,0:T(8,128)(2,1)} %broadcast_in_dim.13), calls=%async_computation.1 | async-start | bytes 786432 | tf_op jit(solution)/shard_map/all_to_all | solution.py:107
  59.1 0.2 fusion.31
  59.3 0.1 reshape.165
  59.3 0.1 copy.52
  59.4 0.1 reshape.184
  59.5 14.7 %all-to-all-done.1 = bf16[8,96,256]{2,1,0:T(8,128)(2,1)S(1)} async-done(((bf16[8,96,256]{2,1,0:T(8,128)(2,1)}), bf16[8,96,256]{2,1,0:T(8,128)(2,1)S(1)}, u32[]{:S(2)}, u32[]{:S(2)}) %all-to-all-start.1) | async-done | bytes 393248 | tf_op jit(solution)/shard_map/all_to_all | solution.py:107
  74.2 0.2 fusion.1
  74.4 0.2 fusion
  74.7 0.1 pad_maximum_fusion
  74.8 0.0 copy-start.1
  74.8 14.7 %all_to_all.25 = bf16[4,256,384]{1,2,0:T(8,128)(2,1)S(1)} all-to-all(bf16[4,256,384]{1,2,0:T(8,128)(2,1)S(1)} %pad_maximum_fusion), channel_id=1, replica_groups=mesh['z'=8,'y'=8,'c'=2,'x'=4] {'x'}, dimensions={0} | all-to-all | bytes 1572864 | tf_op jit(solution)/shard_map/all_to_all | solution.py:107
  89.6 0.3 fusion.11
  90.0 0.5 copy-done.2
  90.4 0.6 convolution_convert_fusion
  91.0 0.2 copy.56
  91.3 11.5 %all_to_all.26 = bf16[4,256,320]{1,2,0:T(8,128)(2,1)S(1)} all-to-all(bf16[4,256,320]{1,2,0:T(8,128)(2,1)S(1)} %pad_maximum_fusion.1), channel_id=1, replica_groups=mesh['z'=8,'y'=8,'c'=2,'x'=4] {'x'}, dimensions={0} | all-to-all | bytes 1310720 | tf_op jit(solution)/shard_map/all_to_all | solution.py:107
  102.7 0.1 slice_reduce_fusion
  102.8 0.1 copy.55
  102.9 0.1 reshape.173
  103.0 0.2 convolution_convert_fusion.2
  103.2 0.1 reshape.175
  103.3 1.0 pad_maximum_fusion.2
  104.3 7.9 %all-to-all-start.4 = ((bf16[128,4,256]{2,1,0:T(4,128)(2,1)}), bf16[128,4,256]{2,1,0:T(4,128)(2,1)S(1)}, u32[]{:S(2)}, u32[]{:S(2)}) async-start(bf16[128,4,256]{2,1,0:T(4,128)(2,1)} %pad_maximum_fusion.2), calls=%async_computation.4 | async-start | bytes 524288 | tf_op jit(solution)/shard_map/all_to_all | solution.py:107
  112.3 0.1 fusion.7
  112.4 15.1 %all-to-all-done.4 = bf16[128,4,256]{2,1,0:T(4,128)(2,1)S(1)} async-done(((bf16[128,4,256]{2,1,0:T(4,128)(2,1)}), bf16[128,4,256]{2,1,0:T(4,128)(2,1)S(1)}, u32[]{:S(2)}, u32[]{:S(2)}) %all-to-all-start.4) | async-done | bytes 262176 | tf_op jit(solution)/shard_map/all_to_all | solution.py:107
  127.6 0.1 slice.63
  127.7 0.1 reshape.185
  127.7 0.2 convert_reduce_fusion.1
  127.9 0.2 fusion.3
  128.1 0.7 add_convert_fusion.1
  (41 shorter events, 0.4 us)
Async XLA Ops:
  0.0 89.9 %copy-start = (bf16[1,128,1024]{2,1,0:T(8,128)(2,1)S(1)}, bf16[1,128,1024]{2,1,0:T(8,128)(2,1)}, u32[]{:S(2)}) copy-start(bf16[1,128,1024]{2,1,0:T(8,128)(2,1)} %param.39) | copy-start | bytes 786436
  2.1 15.9 %copy-start.3 = (bf16[16,1024]{1,0:T(8,128)(2,1)S(1)}, bf16[16,1024]{1,0:T(8,128)(2,1)}, u32[]{:S(2)}) copy-start(bf16[16,1024]{1,0:T(8,128)(2,1)} %hidden_ref.1) | copy-start | bytes 98308
  2.1 16.0 %copy-start.8 = (f32[1024]{0:T(1024)S(1)}, f32[1024]{0:T(1024)}, u32[]{:S(2)}) copy-start(f32[1024]{0:T(1024)} %param.33) | copy-start | bytes 12292
  7.3 32.4 %copy-start.5 = (bf16[32,256]{1,0:T(8,128)(2,1)S(1)}, bf16[32,256]{1,0:T(8,128)(2,1)}, u32[]{:S(2)}) copy-start(bf16[32,256]{1,0:T(8,128)(2,1)} %param.42) | copy-start | bytes 49156
  7.3 32.4 %copy-start.6 = (bf16[32,256]{1,0:T(8,128)(2,1)S(1)}, bf16[32,256]{1,0:T(8,128)(2,1)}, u32[]{:S(2)}) copy-start(bf16[32,256]{1,0:T(8,128)(2,1)} %param.41) | copy-start | bytes 49156
  7.3 32.4 %copy-start.7 = (bf16[32,256]{1,0:T(8,128)(2,1)S(1)}, bf16[32,256]{1,0:T(8,128)(2,1)}, u32[]{:S(2)}) copy-start(bf16[32,256]{1,0:T(8,128)(2,1)} %param.40) | copy-start | bytes 49156
  19.1 35.7 %all-to-all-start = ((bf16[128,4,256]{2,1,0:T(4,128)(2,1)}), bf16[128,4,256]{2,1,0:T(4,128)(2,1)S(1)}, u32[]{:S(2)}, u32[]{:S(2)}) async-start(bf16[128,4,256]{2,1,0:T(4,128)(2,1)} %reshape.164), calls=%async_computation | async-start | bytes 524288 | tf_op jit(solution)/shard_map/all_to_all | solution.py:107
  55.6 18.5 %all-to-all-start.1 = ((bf16[8,96,256]{2,1,0:T(8,128)(2,1)}), bf16[8,96,256]{2,1,0:T(8,128)(2,1)S(1)}, u32[]{:S(2)}, u32[]{:S(2)}) async-start(bf16[8,96,256]{2,1,0:T(8,128)(2,1)} %broadcast_in_dim.13), calls=%async_computation.1 | async-start | bytes 786432 | tf_op jit(solution)/shard_map/all_to_all | solution.py:107
  74.8 14.8 %copy-start.1 = (bf16[1,1024,128]{2,1,0:T(8,128)(2,1)S(1)}, bf16[1,1024,128]{2,1,0:T(8,128)(2,1)}, u32[]{:S(2)}) copy-start(bf16[1,1024,128]{2,1,0:T(8,128)(2,1)} %param.37) | copy-start | bytes 786436
  89.5 1.0 copy-start.2
  102.7 9.5 %copy-start.4 = (s32[16,2]{0,1:T(2,128)S(1)}, s32[16,2]{0,1:T(2,128)}, u32[]{:S(2)}) copy-start(s32[16,2]{0,1:T(2,128)} %param.34) | copy-start | bytes 388
  102.7 9.5 %copy-start.10 = (bf16[1024]{0:T(1024)(128)(2,1)S(1)}, bf16[1024]{0:T(1024)(128)(2,1)}, u32[]{:S(2)}) copy-start(bf16[1024]{0:T(1024)(128)(2,1)} %param.43) | copy-start | bytes 6148
  102.7 9.5 %copy-start.9 = (f32[16,2]{0,1:T(2,128)S(1)}, f32[16,2]{0,1:T(2,128)}, u32[]{:S(2)}) copy-start(f32[16,2]{0,1:T(2,128)} %param.36) | copy-start | bytes 388
  102.7 9.6 %copy-start.11 = (f32[16]{0:T(128)S(1)}, f32[16]{0:T(128)}, u32[]{:S(2)}) copy-start(f32[16]{0:T(128)} %param.35) | copy-start | bytes 196
  104.3 23.3 %all-to-all-start.4 = ((bf16[128,4,256]{2,1,0:T(4,128)(2,1)}), bf16[128,4,256]{2,1,0:T(4,128)(2,1)S(1)}, u32[]{:S(2)}, u32[]{:S(2)}) async-start(bf16[128,4,256]{2,1,0:T(4,128)(2,1)} %pad_maximum_fusion.2), calls=%async_computation.4 | async-start | bytes 524288 | tf_op jit(solution)/shard_map/all_to_all | solution.py:107

commit v3 on v2

--- a/solution.py
+++ b/solution.py
@@ -1,3 +1,5 @@
+import functools
+
 import jax
 import jax.numpy as jnp
 from jax import lax
@@ -25,25 +27,51 @@
 
 def mixer_body(
     hidden_ref,
-    state_ref,
     gain_ref,
-    query_ref,
-    key_ref,
-    value_ref,
     decay_ref,
     beta_ref,
     rate_ref,
     head_gain_ref,
+    query_hbm,
+    key_hbm,
+    value_hbm,
+    out_w_hbm,
+    state_hbm,
+    partial_ref,
+    query_ref,
+    key_ref,
+    value_ref,
     out_w_ref,
-    partial_ref,
+    state_ref,
     read_q,
     read_k,
+    sems,
 ):
     rows, heads, dk, dv = state_ref.shape
+    groups = 4
+    step = rows // groups
+
+    def fetch(source, target, at):
+        return pltpu.make_async_copy(source, target, sems.at[at])
+
+    get_query = fetch(query_hbm, query_ref, 0)
+    get_key = fetch(key_hbm, key_ref, 1)
+    get_value = fetch(value_hbm, value_ref, 2)
+    get_out = fetch(out_w_hbm, out_w_ref, 3)
+    get_state = [
+        fetch(
+            state_hbm.at[pl.ds(g * step, step)], state_ref.at[pl.ds(g * step, step)], 4 + g
+        )
+        for g in range(groups)
+    ]
+    for copy in [get_query, get_key] + get_state + [get_value, get_out]:
+        copy.start()
     wide = hidden_ref[...].astype(F32)
     normed = rms_scale(wide, gain_ref[...], 0.1).astype(BF)
     wide = normed.astype(F32)
+    get_query.wait()
     q_all = dot32(normed, query_ref[...])
+    get_key.wait()
     k_all = dot32(normed, key_ref[...])
     units = []
     for source in (q_all, k_all):
@@ -52,15 +80,18 @@
     used = 2 * heads * rows
     stacked = jnp.concatenate(units + [jnp.zeros((dk - used, dk), F32)], axis=0)
     columns = stacked.T
-    for h in range(heads):
-        for s in range(rows):
-            state = state_ref[s, h]
-            q_col = columns[:, h * rows + s : h * rows + s + 1]
-            k_at = (heads + h) * rows + s
-            k_col = columns[:, k_at : k_at + 1]
-            lanes = slice(h * dv, (h + 1) * dv)
-            read_q[s : s + 1, lanes] = jnp.sum(state * q_col, axis=0, keepdims=True)
-            read_k[s : s + 1, lanes] = jnp.sum(state * k_col, axis=0, keepdims=True)
+    for g in range(groups):
+        get_state[g].wait()
+        for s in range(g * step, (g + 1) * step):
+            for h in range(heads):
+                state = state_ref[s, h]
+                q_col = columns[:, h * rows + s : h * rows + s + 1]
+                k_at = (heads + h) * rows + s
+                k_col = columns[:, k_at : k_at + 1]
+                lanes = slice(h * dv, (h + 1) * dv)
+                read_q[s : s + 1, lanes] = jnp.sum(state * q_col, axis=0, keepdims=True)
+                read_k[s : s + 1, lanes] = jnp.sum(state * k_col, axis=0, keepdims=True)
+    get_value.wait()
     v_all = dot32(normed, value_ref[...])
     outs = []
     for h in range(heads):
@@ -73,6 +104,7 @@
         readout = decay * read_q[:, lanes] + meet * (v_all[:, lanes] - decay * read_k[:, lanes])
         outs.append(rms_scale(readout, head_gain_ref[...], 0.01).astype(BF))
     head_out = jnp.concatenate(outs, axis=1)
+    get_out.wait()
     partial_ref[...] = dot32(head_out, out_w_ref[...]).astype(BF)
 
 
@@ -80,27 +112,161 @@
     rows, width = hidden.shape
     vmem = pl.BlockSpec(memory_space=pltpu.VMEM)
     smem = pl.BlockSpec(memory_space=pltpu.SMEM)
+    hbm = pl.BlockSpec(memory_space=pl.ANY)
     wide = state.shape[1] * state.shape[3]
     return pl.pallas_call(
         mixer_body,
         out_shape=jax.ShapeDtypeStruct((rows, width), BF),
-        in_specs=[vmem] * 8 + [smem] + [vmem] * 2,
+        in_specs=[vmem] * 4 + [smem, vmem] + [hbm] * 5,
         out_specs=vmem,
-        scratch_shapes=[pltpu.VMEM((rows, wide), F32), pltpu.VMEM((rows, wide), F32)],
+        scratch_shapes=[
+            pltpu.VMEM(query.shape, BF),
+            pltpu.VMEM(key.shape, BF),
+            pltpu.VMEM(value.shape, BF),
+            pltpu.VMEM(out_w.shape, BF),
+            pltpu.VMEM(state.shape, F32),
+            pltpu.VMEM((rows, wide), F32),
+            pltpu.VMEM((rows, wide), F32),
+            pltpu.SemaphoreType.DMA((8,)),
+        ],
         name="mixer",
     )(
         hidden,
-        state,
         gain[None],
-        query,
-        key,
-        value,
         decay.T,
         beta.T,
         rate,
         head_gain[None],
+        query,
+        key,
+        value,
         out_w,
-    )
+        state,
+    )
+
+
+def spread_body(*refs):
+    sources, target, sems = refs[:-2], refs[-2], refs[-1]
+    rows = sources[0].shape[0]
+    started = []
+    for c in range(target.shape[0]):
+        for w, source in enumerate(sources):
+            copy = pltpu.make_async_copy(
+                source, target.at[c, pl.ds(w * rows, rows)], sems.at[c * len(sources) + w]
+            )
+            copy.start()
+            started.append(copy)
+    for copy in started:
+        copy.wait()
+
+
+def spread(weights, count):
+    rows, width = weights[0].shape
+    hbm = pl.BlockSpec(memory_space=pl.ANY)
+    return pl.pallas_call(
+        spread_body,
+        out_shape=jax.ShapeDtypeStruct((count, len(weights) * rows, width), BF),
+        in_specs=[hbm] * len(weights),
+        out_specs=hbm,
+        scratch_shapes=[pltpu.SemaphoreType.DMA((count * len(weights),))],
+        name="spread",
+    )(*weights)
+
+
+def prepare_body(
+    n_ep,
+    n_z,
+    tp_ref,
+    partials_ref,
+    hidden_ref,
+    gain_ref,
+    branch_ref,
+    ids_ref,
+    sent_ref,
+    resid_ref,
+    weight_ref,
+    position_ref,
+):
+    rows, width = hidden_ref.shape
+    quarter = resid_ref.shape[1]
+    n_tp = width // quarter
+    choices = ids_ref.shape[0]
+    half = quarter // 2
+    mix = partials_ref[:rows].astype(F32)
+    for t in range(1, n_tp):
+        mix = mix + partials_ref[t * rows : (t + 1) * rows].astype(F32)
+    resid = (hidden_ref[...].astype(F32) + mix).astype(BF).astype(F32)
+    normed = rms_scale(resid, gain_ref[...], 0.1).astype(BF)
+    wide = normed.astype(F32)
+    dot = jnp.sum(wide * branch_ref[...].astype(F32), axis=1, keepdims=True)
+    weight_ref[...] = jnp.broadcast_to(jax.nn.sigmoid(dot), weight_ref.shape)
+    tp_at = tp_ref[0]
+    own = wide[:, :quarter]
+    resid_own = resid[:, :quarter]
+    for t in range(1, n_tp):
+        here = tp_at == t
+        own = jnp.where(here, wide[:, t * quarter : (t + 1) * quarter], own)
+        resid_own = jnp.where(here, resid[:, t * quarter : (t + 1) * quarter], resid_own)
+    resid_ref[...] = resid_own
+
+    row_ids = ids_ref[...].astype(F32)
+    r_at = lax.broadcasted_iota(jnp.int32, (rows, rows), 0)
+    c_at = lax.broadcasted_iota(jnp.int32, (rows, rows), 1)
+    eye = jnp.where(r_at == c_at, 1.0, 0.0)
+    col_ids = lax.dot_general(
+        eye, row_ids, (((1,), (1,)), ((), ())), preferred_element_type=F32
+    )
+    row_pos, col_pos = [], []
+    for j in range(choices):
+        by_row = jnp.zeros((rows, rows), F32)
+        by_col = jnp.zeros((rows, rows), F32)
+        for o in range(choices):
+            by_row += jnp.where(col_ids[:, o : o + 1] == row_ids[j : j + 1, :], 1.0, 0.0)
+            by_col += jnp.where(col_ids[:, j : j + 1] == row_ids[o : o + 1, :], 1.0, 0.0)
+        row_rank = jnp.sum(jnp.where(r_at < c_at, by_row, 0.0), axis=0, keepdims=True)
+        col_rank = jnp.sum(jnp.where(c_at < r_at, by_col, 0.0), axis=1, keepdims=True)
+        row_pos.append(row_ids[j : j + 1, :] * 2.0 + row_rank)
+        col_pos.append(col_ids[:, j : j + 1] * 2.0 + col_rank)
+    lane = lax.broadcasted_iota(jnp.int32, position_ref.shape, 1)
+    position_ref[...] = jnp.where(lane == 0, col_pos[0], col_pos[1]).astype(jnp.int32)
+
+    shape = (n_ep * 8, 2 * rows)
+    at = lax.broadcasted_iota(jnp.int32, shape, 0)
+    col = lax.broadcasted_iota(jnp.int32, shape, 1)
+    slot = at & 1
+    dest = at >> 3
+    expert_key = (dest * 2 + slot).astype(F32)
+    dense_key = (dest // (n_ep // n_z)) * 2 + slot
+    for_expert = (at & 2) == 0
+    same_half = ((at >> 2) & 1) == jnp.where(col >= rows, 1, 0)
+    token = jnp.where(col >= rows, col - rows, col)
+    first = jnp.concatenate([row_pos[0], row_pos[0]], axis=1)
+    second = jnp.concatenate([row_pos[1], row_pos[1]], axis=1)
+    expert_hit = jnp.where(
+        (expert_key == first) | (expert_key == second), 1.0, 0.0
+    )
+    dense_hit = jnp.where(dense_key == token, 1.0, 0.0)
+    pick = jnp.where(same_half, jnp.where(for_expert, expert_hit, dense_hit), 0.0).astype(BF)
+    halves = jnp.concatenate([own[:, :half], own[:, half:]], axis=0).astype(BF)
+    sent_ref[...] = dot32(pick, halves).astype(BF)
+
+
+def prepare(tp_at, partials, hidden, gain, branch_gate, ids, n_ep, n_z, n_tp):
+    rows, width = hidden.shape
+    quarter = width // n_tp
+    vmem = pl.BlockSpec(memory_space=pltpu.VMEM)
+    return pl.pallas_call(
+        functools.partial(prepare_body, n_ep, n_z),
+        out_shape=(
+            jax.ShapeDtypeStruct((n_ep * 8, quarter // 2), BF),
+            jax.ShapeDtypeStruct((rows, quarter), F32),
+            jax.ShapeDtypeStruct((rows, 128), F32),
+            jax.ShapeDtypeStruct((rows, 128), jnp.int32),
+        ),
+        in_specs=[pl.BlockSpec(memory_space=pltpu.SMEM)] + [vmem] * 5,
+        out_specs=(vmem,) * 4,
+        name="prepare",
+    )(tp_at, partials, hidden, gain[None], branch_gate[None], ids.T)
 
 
 def exchange(blocks, axis):
@@ -141,8 +307,7 @@
     tp_at = lax.axis_index("x")
     hid = dense_gate.shape[0]
 
-    dense_all = jnp.concatenate([dense_gate, dense_up, dense_down], axis=0)
-    copies = jnp.broadcast_to(dense_all, (n_z, *dense_all.shape))
+    copies = spread((dense_gate, dense_up, dense_down), n_z)
     dense_z = exchange(copies, "z").reshape(n_z, 3, hid, quarter)
 
     partial_out = mixer(
@@ -158,30 +323,16 @@
         head_gain,
         out_w,
     )
-    partials = lax.all_gather(partial_out, "x")
-    mix = jnp.sum(partials.astype(F32), axis=0)
-    resid = (hidden_in.astype(F32) + mix).astype(BF)
-    normed2 = rms_scale(resid.astype(F32), ffn_gain, 0.1).astype(BF)
-    own = lax.dynamic_slice_in_dim(normed2, tp_at * quarter, quarter, 1)
-    resid_own = lax.dynamic_slice_in_dim(resid, tp_at * quarter, quarter, 1).astype(F32)
-    branch_weight = jax.nn.sigmoid(dot32(normed2, branch_gate))
-    route_weight = (
-        group_share[:, None] * expert_share / jnp.sum(expert_share, axis=1, keepdims=True)
-    )
-
-    same = expert_ids[:, :, None, None] == expert_ids[None, None, :, :]
-    earlier = jnp.arange(rows)[:, None] > jnp.arange(rows)[None, :]
-    rank = jnp.sum(same & earlier[:, None, :, None], axis=(2, 3)).astype(jnp.int32)
-    dest = jnp.arange(n_ep)[:, None, None, None]
-    slot = jnp.arange(cap)[None, :, None, None]
-    chosen = (expert_ids[None, None] == dest) & (rank[None, None] == slot)
-    pick_expert = jnp.any(chosen, axis=3)
-    dense_row = (jnp.arange(n_ep) // (n_ep // n_z))[:, None] * per_z + jnp.arange(per_z)[None, :]
-    pick_dense = dense_row[:, :, None] == jnp.arange(rows)
-    pick = jnp.concatenate([pick_expert, pick_dense], axis=1).astype(BF)
+    partials = lax.all_gather(partial_out, "x", axis=0, tiled=True)
+    sent, resid_own, branch_weight, position = prepare(
+        tp_at[None], partials, hidden_in, ffn_gain, branch_gate, expert_ids, n_ep, n_z, n_tp
+    )
+    branch_weight = branch_weight[:, :1]
+    position = position[:, :2]
     block = cap + per_z
-    sent = dot32(pick.reshape(n_ep * block, rows), own).astype(BF)
-    arrived = exchange(sent.reshape(n_ep, block, quarter), EP)
+    arrived = exchange(sent.reshape(n_ep, 8, quarter // 2), EP)
+    arrived = arrived.reshape(n_ep, 2, block, quarter // 2)
+    arrived = jnp.concatenate([arrived[:, 0], arrived[:, 1]], axis=2)
     moe_rows = arrived[:, :cap].reshape(n_ep * cap, quarter)
     dense_rows = arrived[:, cap:].reshape(n_ep * per_z, quarter)
 
@@ -220,14 +371,16 @@
     returned = exchange(back, EP)
 
     slots = returned[:, :cap].reshape(n_ep * cap, quarter)
-    position = expert_ids * cap + rank
+    route_weight = (
+        group_share[:, None] * expert_share / jnp.sum(expert_share, axis=1, keepdims=True)
+    )
     fetch = (position[:, :, None] == jnp.arange(n_ep * cap)).astype(BF)
     per_choice = dot32(fetch.reshape(rows * 2, n_ep * cap), slots).reshape(rows, 2, quarter)
     moe = jnp.sum(per_choice * route_weight[:, :, None], axis=1)
     branch = jnp.sum(
         returned[:, cap:].astype(F32).reshape(n_z, n_ep // n_z, per_z, quarter), axis=1
     ).reshape(rows, quarter)
-    return (resid_own + moe + branch_weight[:, None] * branch).astype(BF)
+    return (resid_own + moe + branch_weight * branch).astype(BF)
 
 
 def solution(mesh):

time: 129 us -> 134 us (1.039)
  Pallas kernels: 5.19 us -> 21.1 us
  waiting for transfers between devices: 45 us -> 31.6 us
  starting transfers between devices: 31.9 us -> 35.5 us
  other arithmetic: 4.21 us -> 2.34 us
  blocking collectives: 36.7 us -> 38.1 us
    pallas_call x0 -> x2, Pallas kernels: none -> 15.9 us  [the longest x1 13.2 us: spread(): pl.pallas_call(spread_body, out_shape=jax.ShapeDtypeStruct((count, len(we...]
    all_to_all x3, waiting for transfers between devices: 45 us -> 31.6 us  [exchange(): return lax.all_to_all(blocks, axis, split_axis=0, concat_axis=0, tiled=True)]
    all_to_all x3, starting transfers between devices: 31.9 us -> 35.5 us  [exchange(): return lax.all_to_all(blocks, axis, split_axis=0, concat_axis=0, tiled=True)]
    all_gather x1, blocking collectives: 10.6 us -> 12.5 us  [local(): partials = lax.all_gather(partial_out, 'x', axis=0, tiled=True)]
  transfers between devices with their start and end apart: 3 -> 3, of which waited for: 3 -> 3; matrix products, arithmetic and copies ran while one was open for 0% -> 1% of each run, Pallas kernels for 0% -> 10%
where the time goes in v3:
time: 134 us
  blocking collectives  38.1 us (28%)
  starting transfers between devices  35.5 us (26%)
  waiting for transfers between devices  31.6 us (24%)
  Pallas kernels  21.1 us (16%)
  local copies, waits for them, and re-layouts  3.05 us (2%)
  other arithmetic  2.34 us (2%)
  matrix products  1.73 us (1%)
    all_to_all x3, starting transfers between devices, exchange(): return lax.all_to_all(blocks, axis, split_axis=0, concat_axis=0, tiled=True)  35.5 us
    all_to_all x3, waiting for transfers between devices, exchange(): return lax.all_to_all(blocks, axis, split_axis=0, concat_axis=0, tiled=True)  31.6 us
    all_to_all x2, blocking collectives, exchange(): return lax.all_to_all(blocks, axis, split_axis=0, concat_axis=0, tiled=True)  25.6 us
    pallas_call x1, Pallas kernels, spread(): pl.pallas_call(spread_body, out_shape=jax.ShapeDtypeStruct((count, len(we...  13.2 us
    all_gather x1, blocking collectives, local(): partials = lax.all_gather(partial_out, 'x', axis=0, tiled=True)  12.5 us
    pallas_call x1, Pallas kernels, mixer(): pl.pallas_call(mixer_body, out_shape=jax.ShapeDtypeStruct((rows, width),...  5.27 us
  transfers between devices with their start and end apart: 3, of which 3 were waited for; matrix products, arithmetic and copies ran while one was open for 1% of the time, Pallas kernels for 10%

profile of v3, /device:TPU:1, one launch (start us, length us, event | category | flops | bytes accessed | tf_op | source)
XLA Modules:
  0.0 133.6 jit_solution(1814729028878085853)
XLA Ops:
  0.0 0.0 copy-start
  0.0 1.3 broadcast_in_dim.30.branch_ref
  1.3 5.3 %mixer.1 = bf16[16,1024]{1,0:T(8,128)(2,1)} custom-call(bf16[16,1024]{1,0:T(8,128)(2,1)} %hidden_ref.3, f32[1,1024]{1,0:T(1,128)} %bitcast.76, bf16[2,1024]{1,0:T(2,128)(2,1)} %bitcast.77, bf16[2,1024]{1,0:T(2,128)(2,1)} %bitcast.78, f32[2]{0:T(128)} %rate_ref.1, f32[1,128]{1,0:T(1,128)} %bitcast.80, bf16[1024,256]{1,0:T(8,128)(2,1)} %query_hbm.1, ...), custom_call_target="tpu_custom_call" | custom-call | tf_op jit(solution)/shard_map/mixer/pallas_call | solution.py:117
  6.6 12.5 %all_gather.3.partials_ref = bf16[64,1024]{1,0:T(8,128)(2,1)} all-gather(bf16[16,1024]{1,0:T(8,128)(2,1)} %mixer.1), channel_id=1, replica_groups=mesh['z'=8,'y'=8,'c'=2,'x'=4] {'x'}, dimensions={0}, use_global_device_ids=true | all-gather | bytes 163840 | tf_op jit(solution)/shard_map/all_gather | solution.py:326
  19.1 2.7 %prepare.1 = (bf16[1024,128]{1,0:T(8,128)(2,1)}, f32[16,256]{1,0:T(8,128)}, f32[16,128]{1,0:T(8,128)}, s32[16,128]{1,0:T(8,128)}) custom-call(s32[1]{0:T(128)} %bitcast.tp_ref, bf16[64,1024]{1,0:T(8,128)(2,1)} %all_gather.3.partials_ref, bf16[16,1024]{1,0:T(8,128)(2,1)} %hidden_ref.3, f32[1,1024]{1,0:T(1,128)} %bitcast.75, ...), custom_call_target="tpu_custom_call" | custom-call | tf_op jit(solution)/shard_map/prepare/pallas_call | solution.py:258
  21.8 19.7 %all-to-all-start = ((bf16[128,8,128]{2,1,0:T(8,128)(2,1)}), bf16[128,8,128]{2,1,0:T(8,128)(2,1)S(1)}, u32[]{:S(2)}, u32[]{:S(2)}) async-start(bf16[128,8,128]{2,1,0:T(8,128)(2,1)} %bitcast.73), calls=%async_computation | async-start | bytes 524288 | tf_op jit(solution)/shard_map/all_to_all | solution.py:273
  41.5 13.2 %spread.1 = bf16[8,96,256]{2,1,0:T(8,128)(2,1)} custom-call(bf16[32,256]{1,0:T(8,128)(2,1)} %refs_0_.1, bf16[32,256]{1,0:T(8,128)(2,1)} %refs_1_.1, bf16[32,256]{1,0:T(8,128)(2,1)} %refs_2_.1), custom_call_target="tpu_custom_call" | custom-call | tf_op jit(solution)/shard_map/spread/pallas_call | solution.py:166
  54.7 2.0 %all-to-all-done = bf16[128,8,128]{2,1,0:T(8,128)(2,1)S(1)} async-done(((bf16[128,8,128]{2,1,0:T(8,128)(2,1)}), bf16[128,8,128]{2,1,0:T(8,128)(2,1)S(1)}, u32[]{:S(2)}, u32[]{:S(2)}) %all-to-all-start) | async-done | bytes 262176 | tf_op jit(solution)/shard_map/all_to_all | solution.py:273
  56.7 4.9 %all-to-all-start.1 = ((bf16[8,96,256]{2,1,0:T(8,128)(2,1)}), bf16[8,96,256]{2,1,0:T(8,128)(2,1)S(1)}, u32[]{:S(2)}, u32[]{:S(2)}) async-start(bf16[8,96,256]{2,1,0:T(8,128)(2,1)} %spread.1), calls=%async_computation.1 | async-start | bytes 786432 | tf_op jit(solution)/shard_map/all_to_all | solution.py:273
  61.6 0.1 slice_bitcast_fusion.1
  61.7 0.2 fusion.9
  62.0 0.1 reshape.92
  62.0 0.1 copy.42
  62.1 0.1 reshape.109
  62.2 14.6 %all-to-all-done.1 = bf16[8,96,256]{2,1,0:T(8,128)(2,1)S(1)} async-done(((bf16[8,96,256]{2,1,0:T(8,128)(2,1)}), bf16[8,96,256]{2,1,0:T(8,128)(2,1)S(1)}, u32[]{:S(2)}, u32[]{:S(2)}) %all-to-all-start.1) | async-done | bytes 393248 | tf_op jit(solution)/shard_map/all_to_all | solution.py:273
  76.8 0.2 fusion.1
  77.0 0.2 fusion
  77.4 0.1 pad_maximum_fusion
  77.4 0.0 copy-start.1
  77.4 14.1 %all_to_all.25 = bf16[4,256,384]{1,2,0:T(8,128)(2,1)S(1)} all-to-all(bf16[4,256,384]{1,2,0:T(8,128)(2,1)S(1)} %pad_maximum_fusion), channel_id=1, replica_groups=mesh['z'=8,'y'=8,'c'=2,'x'=4] {'x'}, dimensions={0} | all-to-all | bytes 1572864 | tf_op jit(solution)/shard_map/all_to_all | solution.py:273
  91.7 0.0 copy-done.1
  91.7 0.3 fusion.7
  92.0 0.0 copy-done
  92.0 0.5 copy-done.2
  92.5 0.5 convolution_convert_fusion
  93.0 0.2 copy.46
  93.3 11.5 %all_to_all.26 = bf16[4,256,320]{1,2,0:T(8,128)(2,1)S(1)} all-to-all(bf16[4,256,320]{1,2,0:T(8,128)(2,1)S(1)} %pad_maximum_fusion.1), channel_id=1, replica_groups=mesh['z'=8,'y'=8,'c'=2,'x'=4] {'x'}, dimensions={0} | all-to-all | bytes 1310720 | tf_op jit(solution)/shard_map/all_to_all | solution.py:273
  104.8 0.1 slice_reduce_fusion
  104.9 0.1 copy.45
  105.0 0.0 copy-start.3
  105.0 0.1 reshape.100
  105.1 0.2 convolution_convert_fusion.1
  105.3 0.1 reshape.102
  105.4 1.0 pad_maximum_fusion.2
  106.3 10.8 %all-to-all-start.4 = ((bf16[128,4,256]{2,1,0:T(4,128)(2,1)}), bf16[128,4,256]{2,1,0:T(4,128)(2,1)S(1)}, u32[]{:S(2)}, u32[]{:S(2)}) async-start(bf16[128,4,256]{2,1,0:T(4,128)(2,1)} %pad_maximum_fusion.2), calls=%async_computation.4 | async-start | bytes 524288 | tf_op jit(solution)/shard_map/all_to_all | solution.py:273
  117.2 0.0 copy-done.4
  117.2 0.1 copy.39
  117.3 0.0 copy-done.6
  117.3 0.0 copy-done.5
  117.3 0.1 slice_reduce_fusion.1
  117.4 0.0 copy-done.7
  117.4 15.0 %all-to-all-done.4 = bf16[128,4,256]{2,1,0:T(4,128)(2,1)S(1)} async-done(((bf16[128,4,256]{2,1,0:T(4,128)(2,1)}), bf16[128,4,256]{2,1,0:T(4,128)(2,1)S(1)}, u32[]{:S(2)}, u32[]{:S(2)}) %all-to-all-start.4) | async-done | bytes 262176 | tf_op jit(solution)/shard_map/all_to_all | solution.py:273
  132.4 0.1 slice.81
  132.5 0.1 reshape.110
  132.6 0.2 convert_reduce_fusion.1
  132.8 0.2 fusion.3
  132.9 0.0 copy-done.3
  133.0 0.7 add_convert_fusion
  (18 shorter events, 0.3 us)
Async XLA Ops:
  0.0 92.0 %copy-start = (bf16[1,128,1024]{2,1,0:T(8,128)(2,1)S(1)}, bf16[1,128,1024]{2,1,0:T(8,128)(2,1)}, u32[]{:S(2)}) copy-start(bf16[1,128,1024]{2,1,0:T(8,128)(2,1)} %param.39) | copy-start | bytes 786436
  21.8 35.0 %all-to-all-start = ((bf16[128,8,128]{2,1,0:T(8,128)(2,1)}), bf16[128,8,128]{2,1,0:T(8,128)(2,1)S(1)}, u32[]{:S(2)}, u32[]{:S(2)}) async-start(bf16[128,8,128]{2,1,0:T(8,128)(2,1)} %bitcast.73), calls=%async_computation | async-start | bytes 524288 | tf_op jit(solution)/shard_map/all_to_all | solution.py:273
  56.7 20.0 %all-to-all-start.1 = ((bf16[8,96,256]{2,1,0:T(8,128)(2,1)}), bf16[8,96,256]{2,1,0:T(8,128)(2,1)S(1)}, u32[]{:S(2)}, u32[]{:S(2)}) async-start(bf16[8,96,256]{2,1,0:T(8,128)(2,1)} %spread.1), calls=%async_computation.1 | async-start | bytes 786432 | tf_op jit(solution)/shard_map/all_to_all | solution.py:273
  77.4 14.2 %copy-start.1 = (bf16[1,1024,128]{2,1,0:T(8,128)(2,1)S(1)}, bf16[1,1024,128]{2,1,0:T(8,128)(2,1)}, u32[]{:S(2)}) copy-start(bf16[1,1024,128]{2,1,0:T(8,128)(2,1)} %param.37) | copy-start | bytes 786436
  91.5 1.0 copy-start.2
  104.8 12.4 %copy-start.4 = (s32[16,128]{1,0:T(8,128)S(1)}, s32[16,128]{1,0:T(8,128)}, u32[]{:S(2)}) copy-start(s32[16,128]{1,0:T(8,128)} %get-tuple-element.10) | copy-start | bytes 24580
  104.8 12.5 %copy-start.6 = (f32[16,2]{0,1:T(2,128)S(1)}, f32[16,2]{0,1:T(2,128)}, u32[]{:S(2)}) copy-start(f32[16,2]{0,1:T(2,128)} %param.36) | copy-start | bytes 388
  104.8 12.5 %copy-start.5 = (f32[16,128]{1,0:T(8,128)S(1)}, f32[16,128]{1,0:T(8,128)}, u32[]{:S(2)}) copy-start(f32[16,128]{1,0:T(8,128)} %get-tuple-element.12) | copy-start | bytes 24580
  104.8 12.6 %copy-start.7 = (f32[16]{0:T(128)S(1)}, f32[16]{0:T(128)}, u32[]{:S(2)}) copy-start(f32[16]{0:T(128)} %param.35) | copy-start | bytes 196
  105.0 28.0 %copy-start.3 = (f32[16,256]{1,0:T(8,128)S(1)}, f32[16,256]{1,0:T(8,128)}, u32[]{:S(2)}) copy-start(f32[16,256]{1,0:T(8,128)} %get-tuple-element.9) | copy-start | bytes 49156
  106.3 26.1 %all-to-all-start.4 = ((bf16[128,4,256]{2,1,0:T(4,128)(2,1)}), bf16[128,4,256]{2,1,0:T(4,128)(2,1)S(1)}, u32[]{:S(2)}, u32[]{:S(2)}) async-start(bf16[128,4,256]{2,1,0:T(4,128)(2,1)} %pad_maximum_fusion.2), calls=%async_computation.4 | async-start | bytes 524288 | tf_op jit(solution)/shard_map/all_to_all | solution.py:273

commit v4 on v2

--- a/solution.py
+++ b/solution.py
@@ -23,44 +23,98 @@
     return jnp.dot(a, b, preferred_element_type=F32)
 
 
+def slots_of(ids_ref, row_slot_ref, col_slot_ref, rows):
+    choices = ids_ref.shape[0]
+    row_ids = ids_ref[...].astype(F32)
+    r_at = lax.broadcasted_iota(jnp.int32, (rows, rows), 0)
+    c_at = lax.broadcasted_iota(jnp.int32, (rows, rows), 1)
+    eye = jnp.where(r_at == c_at, 1.0, 0.0)
+    col_ids = lax.dot_general(eye, row_ids, (((1,), (1,)), ((), ())), preferred_element_type=F32)
+    row_slots, col_slots = [], []
+    for j in range(choices):
+        by_row = jnp.zeros((rows, rows), F32)
+        by_col = jnp.zeros((rows, rows), F32)
+        for o in range(choices):
+            by_row += jnp.where(col_ids[:, o : o + 1] == row_ids[j : j + 1, :], 1.0, 0.0)
+            by_col += jnp.where(col_ids[:, j : j + 1] == row_ids[o : o + 1, :], 1.0, 0.0)
+        row_rank = jnp.sum(jnp.where(r_at < c_at, by_row, 0.0), axis=0, keepdims=True)
+        col_rank = jnp.sum(jnp.where(c_at < r_at, by_col, 0.0), axis=1, keepdims=True)
+        row_slots.append(row_ids[j : j + 1, :] * 2.0 + row_rank)
+        col_slots.append(col_ids[:, j : j + 1] * 2.0 + col_rank)
+    row_slot_ref[...] = jnp.concatenate(row_slots, axis=0).astype(jnp.int32)
+    col_slot_ref[...] = jnp.concatenate(col_slots, axis=1).astype(jnp.int32)
+
+
 def mixer_body(
     hidden_ref,
-    state_ref,
     gain_ref,
-    query_ref,
-    key_ref,
-    value_ref,
     decay_ref,
     beta_ref,
     rate_ref,
     head_gain_ref,
+    ids_ref,
+    query_hbm,
+    key_hbm,
+    value_hbm,
+    out_w_hbm,
+    state_hbm,
+    partial_ref,
+    row_slot_ref,
+    col_slot_ref,
+    query_ref,
+    key_ref,
+    value_ref,
     out_w_ref,
-    partial_ref,
-    read_q,
-    read_k,
+    state_ref,
+    sems,
 ):
-    rows, heads, dk, dv = state_ref.shape
+    rows = hidden_ref.shape[0]
+    heads = decay_ref.shape[0]
+    dv = head_gain_ref.shape[1]
+    dk = query_ref.shape[1] // heads
+    groups = 4
+    step = state_ref.shape[0] // groups
+
+    def fetch(source, target, at):
+        return pltpu.make_async_copy(source, target, sems.at[at])
+
+    get_query = fetch(query_hbm, query_ref, 0)
+    get_key = fetch(key_hbm, key_ref, 1)
+    get_value = fetch(value_hbm, value_ref, 2)
+    get_out = fetch(out_w_hbm, out_w_ref, 3)
+    get_state = [
+        fetch(
+            state_hbm.at[pl.ds(g * step, step)], state_ref.at[pl.ds(g * step, step)], 4 + g
+        )
+        for g in range(groups)
+    ]
+    for copy in [get_query, get_key] + get_state + [get_value, get_out]:
+        copy.start()
+    slots_of(ids_ref, row_slot_ref, col_slot_ref, rows)
     wide = hidden_ref[...].astype(F32)
     normed = rms_scale(wide, gain_ref[...], 0.1).astype(BF)
     wide = normed.astype(F32)
+    get_query.wait()
     q_all = dot32(normed, query_ref[...])
+    get_key.wait()
     k_all = dot32(normed, key_ref[...])
     units = []
     for source in (q_all, k_all):
         for h in range(heads):
             units.append(unit_rows(source[:, h * dk : (h + 1) * dk]))
-    used = 2 * heads * rows
-    stacked = jnp.concatenate(units + [jnp.zeros((dk - used, dk), F32)], axis=0)
-    columns = stacked.T
-    for h in range(heads):
-        for s in range(rows):
-            state = state_ref[s, h]
-            q_col = columns[:, h * rows + s : h * rows + s + 1]
-            k_at = (heads + h) * rows + s
-            k_col = columns[:, k_at : k_at + 1]
-            lanes = slice(h * dv, (h + 1) * dv)
-            read_q[s : s + 1, lanes] = jnp.sum(state * q_col, axis=0, keepdims=True)
-            read_k[s : s + 1, lanes] = jnp.sum(state * k_col, axis=0, keepdims=True)
+    stacked = jnp.concatenate(units, axis=0).astype(BF)
+    pairs = heads * rows
+    row_at = lax.broadcasted_iota(jnp.int32, stacked.shape, 0) % pairs
+    zero = jnp.zeros_like(stacked)
+    read = jnp.zeros((2 * pairs, dv), F32)
+    for g in range(groups):
+        get_state[g].wait()
+        blocks = []
+        for b in range(g * step // dk, (g + 1) * step // dk):
+            blocks.append(jnp.where(row_at == (b % heads) * rows + b // heads, stacked, zero))
+        state = state_ref[g * step : (g + 1) * step].astype(BF)
+        read = read + dot32(jnp.concatenate(blocks, axis=1), state)
+    get_value.wait()
     v_all = dot32(normed, value_ref[...])
     outs = []
     for h in range(heads):
@@ -70,37 +124,73 @@
         decay = jnp.exp(-rate_ref[h] * jax.nn.softplus(decay_in))
         meet = jnp.sum(units[h] * units[heads + h], axis=1, keepdims=True)
         meet = meet * jax.nn.sigmoid(beta_in)
-        readout = decay * read_q[:, lanes] + meet * (v_all[:, lanes] - decay * read_k[:, lanes])
+        read_q = read[h * rows : (h + 1) * rows]
+        read_k = read[pairs + h * rows : pairs + (h + 1) * rows]
+        readout = decay * read_q + meet * (v_all[:, lanes] - decay * read_k)
         outs.append(rms_scale(readout, head_gain_ref[...], 0.01).astype(BF))
     head_out = jnp.concatenate(outs, axis=1)
+    get_out.wait()
     partial_ref[...] = dot32(head_out, out_w_ref[...]).astype(BF)
 
 
-def mixer(hidden, state, gain, query, key, value, decay, beta, rate, head_gain, out_w):
+def mixer(hidden, state, gain, query, key, value, decay, beta, rate, head_gain, out_w, ids):
     rows, width = hidden.shape
     vmem = pl.BlockSpec(memory_space=pltpu.VMEM)
     smem = pl.BlockSpec(memory_space=pltpu.SMEM)
-    wide = state.shape[1] * state.shape[3]
+    hbm = pl.BlockSpec(memory_space=pl.ANY)
+    state = state.reshape(-1, state.shape[-1])
     return pl.pallas_call(
         mixer_body,
-        out_shape=jax.ShapeDtypeStruct((rows, width), BF),
-        in_specs=[vmem] * 8 + [smem] + [vmem] * 2,
-        out_specs=vmem,
-        scratch_shapes=[pltpu.VMEM((rows, wide), F32), pltpu.VMEM((rows, wide), F32)],
+        out_shape=(
+            jax.ShapeDtypeStruct((rows, width), BF),
+            jax.ShapeDtypeStruct(ids.shape[::-1], jnp.int32),
+            jax.ShapeDtypeStruct(ids.shape, jnp.int32),
+        ),
+        in_specs=[vmem] * 4 + [smem, vmem, vmem] + [hbm] * 5,
+        out_specs=(vmem,) * 3,
+        scratch_shapes=[
+            pltpu.VMEM(query.shape, BF),
+            pltpu.VMEM(key.shape, BF),
+            pltpu.VMEM(value.shape, BF),
+            pltpu.VMEM(out_w.shape, BF),
+            pltpu.VMEM(state.shape, F32),
+            pltpu.SemaphoreType.DMA((8,)),
+        ],
         name="mixer",
     )(
         hidden,
-        state,
         gain[None],
-        query,
-        key,
-        value,
         decay.T,
         beta.T,
         rate,
         head_gain[None],
+        ids.T,
+        query,
+        key,
+        value,
         out_w,
-    )
+        state,
+    )
+
+
+def spread_body(*refs):
+    sources, target = refs[:-1], refs[-1]
+    rows = sources[0].shape[0]
+    for w, source in enumerate(sources):
+        for c in range(target.shape[0]):
+            target[c, w * rows : (w + 1) * rows, :] = source[...]
+
+
+def spread(weights, count):
+    rows, width = weights[0].shape
+    vmem = pl.BlockSpec(memory_space=pltpu.VMEM)
+    return pl.pallas_call(
+        spread_body,
+        out_shape=jax.ShapeDtypeStruct((count, len(weights) * rows, width), BF),
+        in_specs=[vmem] * len(weights),
+        out_specs=vmem,
+        name="spread",
+    )(*weights)
 
 
 def exchange(blocks, axis):
@@ -141,11 +231,10 @@
     tp_at = lax.axis_index("x")
     hid = dense_gate.shape[0]
 
-    dense_all = jnp.concatenate([dense_gate, dense_up, dense_down], axis=0)
-    copies = jnp.broadcast_to(dense_all, (n_z, *dense_all.shape))
+    copies = spread((dense_gate, dense_up, dense_down), n_z)
     dense_z = exchange(copies, "z").reshape(n_z, 3, hid, quarter)
 
-    partial_out = mixer(
+    partial_out, row_slot, position = mixer(
         hidden_in,
         prior_state,
         mix_gain,
@@ -157,31 +246,32 @@
         decay_rate,
         head_gain,
         out_w,
-    )
-    partials = lax.all_gather(partial_out, "x")
+        expert_ids,
+    )
+    partials = lax.all_gather(partial_out, "x", axis=0, tiled=True)
+    partials = partials.reshape(n_tp, rows, width)
     mix = jnp.sum(partials.astype(F32), axis=0)
     resid = (hidden_in.astype(F32) + mix).astype(BF)
     normed2 = rms_scale(resid.astype(F32), ffn_gain, 0.1).astype(BF)
     own = lax.dynamic_slice_in_dim(normed2, tp_at * quarter, quarter, 1)
     resid_own = lax.dynamic_slice_in_dim(resid, tp_at * quarter, quarter, 1).astype(F32)
-    branch_weight = jax.nn.sigmoid(dot32(normed2, branch_gate))
-    route_weight = (
-        group_share[:, None] * expert_share / jnp.sum(expert_share, axis=1, keepdims=True)
-    )
-
-    same = expert_ids[:, :, None, None] == expert_ids[None, None, :, :]
-    earlier = jnp.arange(rows)[:, None] > jnp.arange(rows)[None, :]
-    rank = jnp.sum(same & earlier[:, None, :, None], axis=(2, 3)).astype(jnp.int32)
-    dest = jnp.arange(n_ep)[:, None, None, None]
-    slot = jnp.arange(cap)[None, :, None, None]
-    chosen = (expert_ids[None, None] == dest) & (rank[None, None] == slot)
-    pick_expert = jnp.any(chosen, axis=3)
-    dense_row = (jnp.arange(n_ep) // (n_ep // n_z))[:, None] * per_z + jnp.arange(per_z)[None, :]
-    pick_dense = dense_row[:, :, None] == jnp.arange(rows)
-    pick = jnp.concatenate([pick_expert, pick_dense], axis=1).astype(BF)
+    branch_weight = jax.nn.sigmoid(dot32(normed2, branch_gate))[:, None]
+
     block = cap + per_z
-    sent = dot32(pick.reshape(n_ep * block, rows), own).astype(BF)
-    arrived = exchange(sent.reshape(n_ep, block, quarter), EP)
+    at = jnp.arange(n_ep * 2 * block)[:, None]
+    dest, slot = at // (2 * block), at % cap
+    col = jnp.arange(2 * rows)[None, :]
+    slots = jnp.concatenate([row_slot, row_slot], axis=1)
+    expert_at = dest * cap + slot
+    expert_hit = (slots[:1] == expert_at) | (slots[1:] == expert_at)
+    dense_hit = col % rows == dest // (n_ep // n_z) * per_z + slot
+    hit = jnp.where(at % block < cap, expert_hit, dense_hit)
+    pick = (hit & (at % (2 * block) // block == col // rows)).astype(BF)
+    halves = jnp.concatenate([own[:, : quarter // 2], own[:, quarter // 2 :]], axis=0)
+    sent = dot32(pick, halves).astype(BF)
+    arrived = exchange(sent.reshape(n_ep, 8, quarter // 2), EP)
+    arrived = arrived.reshape(n_ep, 2, block, quarter // 2)
+    arrived = jnp.concatenate([arrived[:, 0], arrived[:, 1]], axis=2)
     moe_rows = arrived[:, :cap].reshape(n_ep * cap, quarter)
     dense_rows = arrived[:, cap:].reshape(n_ep * per_z, quarter)
 
@@ -220,14 +310,16 @@
     returned = exchange(back, EP)
 
     slots = returned[:, :cap].reshape(n_ep * cap, quarter)
-    position = expert_ids * cap + rank
+    route_weight = (
+        group_share[:, None] * expert_share / jnp.sum(expert_share, axis=1, keepdims=True)
+    )
     fetch = (position[:, :, None] == jnp.arange(n_ep * cap)).astype(BF)
     per_choice = dot32(fetch.reshape(rows * 2, n_ep * cap), slots).reshape(rows, 2, quarter)
     moe = jnp.sum(per_choice * route_weight[:, :, None], axis=1)
     branch = jnp.sum(
         returned[:, cap:].astype(F32).reshape(n_z, n_ep // n_z, per_z, quarter), axis=1
     ).reshape(rows, quarter)
-    return (resid_own + moe + branch_weight[:, None] * branch).astype(BF)
+    return (resid_own + moe + branch_weight * branch).astype(BF)
 
 
 def solution(mesh):

time: 129 us -> 127 us (0.984)
  waiting for transfers between devices: 45 us -> 43.3 us
  local copies, waits for them, and re-layouts: 3.33 us -> 1.63 us
  matrix products: 2.06 us -> 3.66 us
    all_to_all x3, waiting for transfers between devices: 45 us -> 43.3 us  [exchange(): return lax.all_to_all(blocks, axis, split_axis=0, concat_axis=0, tiled=True)]
    dot_general x6, matrix products: 1.63 us -> 3.22 us  [dot32(): return jnp.dot(a, b, preferred_element_type=F32)]
    pallas_call x1 -> x2, Pallas kernels: 5.19 us -> 5.9 us  [the longest x1 4.36 us: mixer(): pl.pallas_call(mixer_body, out_shape=(jax.ShapeDtypeStruct((rows, width),...]
  transfers between devices with their start and end apart: 3 -> 3, of which waited for: 3 -> 3; matrix products, arithmetic and copies ran while one was open for 0% -> 1% of each run, Pallas kernels for 0% -> 1%
where the time goes in v4:
time: 127 us
  waiting for transfers between devices  43.3 us (34%)
  blocking collectives  36.6 us (29%)
  starting transfers between devices  31.8 us (25%)
  Pallas kernels  5.9 us (5%)
  matrix products  3.66 us (3%)
  other arithmetic  3.43 us (3%)
  local copies, waits for them, and re-layouts  1.63 us (1%)
    all_to_all x3, waiting for transfers between devices, exchange(): return lax.all_to_all(blocks, axis, split_axis=0, concat_axis=0, tiled=True)  43.3 us
    all_to_all x3, starting transfers between devices, exchange(): return lax.all_to_all(blocks, axis, split_axis=0, concat_axis=0, tiled=True)  31.8 us
    all_to_all x2, blocking collectives, exchange(): return lax.all_to_all(blocks, axis, split_axis=0, concat_axis=0, tiled=True)  26.1 us
    all_gather x1, blocking collectives, local(): partials = lax.all_gather(partial_out, 'x', axis=0, tiled=True)  10.5 us
    pallas_call x1, Pallas kernels, mixer(): pl.pallas_call(mixer_body, out_shape=(jax.ShapeDtypeStruct((rows, width),...  4.36 us
    dot_general x6, matrix products, dot32(): return jnp.dot(a, b, preferred_element_type=F32)  3.22 us
  transfers between devices with their start and end apart: 3, of which 3 were waited for; matrix products, arithmetic and copies ran while one was open for 1% of the time, Pallas kernels for 1%

profile of v4, /device:TPU:1, one launch (start us, length us, event | category | flops | bytes accessed | tf_op | source)
XLA Modules:
  0.0 126.7 jit_solution(15935583865980412677)
XLA Ops:
  0.0 0.0 copy-start
  0.1 0.0 copy-start.3
  0.1 0.0 copy-start.5
  0.1 4.4 %mixer.1 = (bf16[16,1024]{1,0:T(8,128)(2,1)}, s32[2,16]{1,0:T(2,128)}, s32[16,2]{1,0:T(8,128)}) custom-call(bf16[16,1024]{1,0:T(8,128)(2,1)} %hidden_ref.1, f32[1,1024]{1,0:T(1,128)} %bitcast.92, bf16[2,1024]{1,0:T(2,128)(2,1)} %bitcast.93, bf16[2,1024]{1,0:T(2,128)(2,1)} %bitcast.94, f32[2]{0:T(128)} %rate_ref.1, f32[1,128]{1,0:T(1,128)} %bitcast.96, ...), custom_call_target="tpu_custom_call" | custom-call | tf_op jit(solution)/shard_map/mixer/pallas_call | solution.py:142
  4.5 0.8 pad_add_fusion
  5.3 10.5 %all_gather.3 = bf16[64,1024]{1,0:T(8,128)(2,1)S(1)} all-gather(bf16[16,1024]{1,0:T(8,128)(2,1)} %get-tuple-element.8), channel_id=1, replica_groups=mesh['z'=8,'y'=8,'c'=2,'x'=4] {'x'}, dimensions={0}, use_global_device_ids=true | all-gather | bytes 163840 | tf_op jit(solution)/shard_map/all_gather | solution.py:251
  15.8 0.0 copy-done.3
  15.8 0.1 fusion.35
  15.9 0.0 copy-done.5
  15.9 0.1 fusion.37
  16.0 1.8 %fusion = bf16[128,8,128]{2,1,0:T(8,128)(2,1)} fusion(s32[32]{0:T(128)S(1)} %get-tuple-element.24, s32[32]{0:T(128)S(1)} %get-tuple-element.25, s32[32]{0:T(128)S(1)} %get-tuple-element.23, s32[32]{0:T(128)S(1)} %get-tuple-element.22, s32[1024]{0:T(1024)S(1)} %get-tuple-element.26, s32[1024]{0:T(1024)S(1)} %get-tuple-element.27, s32[1024]{0:T(1024)S(1)} %fusion.61, ...), kind=kOutput, calls=%fused_computation.2 | convolution fusion | flops 8765440 | bytes 284160 | tf_op jit(solution)/shard_map/dot_general | solution.py:23
  17.8 20.5 %all-to-all-start = ((bf16[128,8,128]{2,1,0:T(8,128)(2,1)}), bf16[128,8,128]{2,1,0:T(8,128)(2,1)S(1)}, u32[]{:S(2)}, u32[]{:S(2)}) async-start(bf16[128,8,128]{2,1,0:T(8,128)(2,1)} %fusion), calls=%async_computation | async-start | bytes 524288 | tf_op jit(solution)/shard_map/all_to_all | solution.py:197
  38.3 1.5 %spread.1 = bf16[8,96,256]{2,1,0:T(8,128)(2,1)} custom-call(bf16[32,256]{1,0:T(8,128)(2,1)} %refs_0_.1, bf16[32,256]{1,0:T(8,128)(2,1)} %refs_1_.1, bf16[32,256]{1,0:T(8,128)(2,1)} %refs_2_.1), custom_call_target="tpu_custom_call" | custom-call | tf_op jit(solution)/shard_map/spread/pallas_call | solution.py:187
  39.8 13.7 %all-to-all-done = bf16[128,8,128]{2,1,0:T(8,128)(2,1)S(1)} async-done(((bf16[128,8,128]{2,1,0:T(8,128)(2,1)}), bf16[128,8,128]{2,1,0:T(8,128)(2,1)S(1)}, u32[]{:S(2)}, u32[]{:S(2)}) %all-to-all-start) | async-done | bytes 262176 | tf_op jit(solution)/shard_map/all_to_all | solution.py:197
  53.5 3.5 %all-to-all-start.1 = ((bf16[8,96,256]{2,1,0:T(8,128)(2,1)}), bf16[8,96,256]{2,1,0:T(8,128)(2,1)S(1)}, u32[]{:S(2)}, u32[]{:S(2)}) async-start(bf16[8,96,256]{2,1,0:T(8,128)(2,1)} %spread.1), calls=%async_computation.1 | async-start | bytes 786432 | tf_op jit(solution)/shard_map/all_to_all | solution.py:197
  57.0 0.1 slice_bitcast_fusion.1
  57.1 0.2 fusion.29
  57.3 0.1 reshape.319
  57.4 0.1 copy.42
  57.5 0.1 reshape.337
  57.6 14.5 %all-to-all-done.1 = bf16[8,96,256]{2,1,0:T(8,128)(2,1)S(1)} async-done(((bf16[8,96,256]{2,1,0:T(8,128)(2,1)}), bf16[8,96,256]{2,1,0:T(8,128)(2,1)S(1)}, u32[]{:S(2)}, u32[]{:S(2)}) %all-to-all-start.1) | async-done | bytes 393248 | tf_op jit(solution)/shard_map/all_to_all | solution.py:197
  72.1 0.2 fusion.2
  72.3 0.2 fusion.1
  72.6 0.1 pad_maximum_fusion
  72.7 0.0 copy-start.1
  72.7 14.7 %all_to_all.25 = bf16[4,256,384]{1,2,0:T(8,128)(2,1)S(1)} all-to-all(bf16[4,256,384]{1,2,0:T(8,128)(2,1)S(1)} %pad_maximum_fusion), channel_id=1, replica_groups=mesh['z'=8,'y'=8,'c'=2,'x'=4] {'x'}, dimensions={0} | all-to-all | bytes 1572864 | tf_op jit(solution)/shard_map/all_to_all | solution.py:197
  87.5 0.3 fusion.19
  87.9 0.5 copy-done.2
  88.3 0.5 convolution_convert_fusion
  88.9 0.2 copy.46
  89.2 11.5 %all_to_all.26 = bf16[4,256,320]{1,2,0:T(8,128)(2,1)S(1)} all-to-all(bf16[4,256,320]{1,2,0:T(8,128)(2,1)S(1)} %pad_maximum_fusion.1), channel_id=1, replica_groups=mesh['z'=8,'y'=8,'c'=2,'x'=4] {'x'}, dimensions={0} | all-to-all | bytes 1310720 | tf_op jit(solution)/shard_map/all_to_all | solution.py:197
  100.7 0.1 slice_reduce_fusion
  100.7 0.1 copy.45
  100.9 0.1 reshape.327
  100.9 0.2 convolution_convert_fusion.2
  101.2 0.1 reshape.329
  101.2 1.0 pad_maximum_fusion.2
  102.2 7.9 %all-to-all-start.4 = ((bf16[128,4,256]{2,1,0:T(4,128)(2,1)}), bf16[128,4,256]{2,1,0:T(4,128)(2,1)S(1)}, u32[]{:S(2)}, u32[]{:S(2)}) async-start(bf16[128,4,256]{2,1,0:T(4,128)(2,1)} %pad_maximum_fusion.2), calls=%async_computation.4 | async-start | bytes 524288 | tf_op jit(solution)/shard_map/all_to_all | solution.py:197
  110.1 0.0 copy-done.7
  110.1 0.1 copy.39
  110.2 0.0 copy-done.6
  110.3 0.1 fusion.8
  110.4 15.1 %all-to-all-done.4 = bf16[128,4,256]{2,1,0:T(4,128)(2,1)S(1)} async-done(((bf16[128,4,256]{2,1,0:T(4,128)(2,1)}), bf16[128,4,256]{2,1,0:T(4,128)(2,1)S(1)}, u32[]{:S(2)}, u32[]{:S(2)}) %all-to-all-start.4) | async-done | bytes 262176 | tf_op jit(solution)/shard_map/all_to_all | solution.py:197
  125.5 0.1 slice.89
  125.5 0.1 reshape.338
  125.6 0.2 convert_reduce_fusion.1
  125.8 0.2 fusion.4
  126.0 0.7 add_convert_fusion.1
  (31 shorter events, 0.4 us)
Async XLA Ops:
  0.0 87.9 %copy-start = (bf16[1,128,1024]{2,1,0:T(8,128)(2,1)S(1)}, bf16[1,128,1024]{2,1,0:T(8,128)(2,1)}, u32[]{:S(2)}) copy-start(bf16[1,128,1024]{2,1,0:T(8,128)(2,1)} %param.39) | copy-start | bytes 786436
  0.1 15.7 %copy-start.3 = (bf16[16,1024]{1,0:T(8,128)(2,1)S(1)}, bf16[16,1024]{1,0:T(8,128)(2,1)}, u32[]{:S(2)}) copy-start(bf16[16,1024]{1,0:T(8,128)(2,1)} %hidden_ref.1) | copy-start | bytes 98308
  0.1 15.8 %copy-start.5 = (f32[1024]{0:T(1024)S(1)}, f32[1024]{0:T(1024)}, u32[]{:S(2)}) copy-start(f32[1024]{0:T(1024)} %param.33) | copy-start | bytes 12292
  17.8 35.7 %all-to-all-start = ((bf16[128,8,128]{2,1,0:T(8,128)(2,1)}), bf16[128,8,128]{2,1,0:T(8,128)(2,1)S(1)}, u32[]{:S(2)}, u32[]{:S(2)}) async-start(bf16[128,8,128]{2,1,0:T(8,128)(2,1)} %fusion), calls=%async_computation | async-start | bytes 524288 | tf_op jit(solution)/shard_map/all_to_all | solution.py:197
  53.5 18.5 %all-to-all-start.1 = ((bf16[8,96,256]{2,1,0:T(8,128)(2,1)}), bf16[8,96,256]{2,1,0:T(8,128)(2,1)S(1)}, u32[]{:S(2)}, u32[]{:S(2)}) async-start(bf16[8,96,256]{2,1,0:T(8,128)(2,1)} %spread.1), calls=%async_computation.1 | async-start | bytes 786432 | tf_op jit(solution)/shard_map/all_to_all | solution.py:197
  72.7 14.8 %copy-start.1 = (bf16[1,1024,128]{2,1,0:T(8,128)(2,1)S(1)}, bf16[1,1024,128]{2,1,0:T(8,128)(2,1)}, u32[]{:S(2)}) copy-start(bf16[1,1024,128]{2,1,0:T(8,128)(2,1)} %param.37) | copy-start | bytes 786436
  87.4 1.0 copy-start.2
  100.7 9.5 %copy-start.7 = (bf16[1024]{0:T(1024)(128)(2,1)S(1)}, bf16[1024]{0:T(1024)(128)(2,1)}, u32[]{:S(2)}) copy-start(bf16[1024]{0:T(1024)(128)(2,1)} %param.43) | copy-start | bytes 6148
  100.7 9.5 %copy-start.4 = (s32[16,2]{1,0:T(8,128)S(1)}, s32[16,2]{1,0:T(8,128)}, u32[]{:S(2)}) copy-start(s32[16,2]{1,0:T(8,128)} %get-tuple-element.9) | copy-start | bytes 388
  100.7 9.6 %copy-start.6 = (f32[16,2]{0,1:T(2,128)S(1)}, f32[16,2]{0,1:T(2,128)}, u32[]{:S(2)}) copy-start(f32[16,2]{0,1:T(2,128)} %param.36) | copy-start | bytes 388
  100.7 9.6 %copy-start.8 = (f32[16]{0:T(128)S(1)}, f32[16]{0:T(128)}, u32[]{:S(2)}) copy-start(f32[16]{0:T(128)} %param.35) | copy-start | bytes 196
  102.2 23.3 %all-to-all-start.4 = ((bf16[128,4,256]{2,1,0:T(4,128)(2,1)}), bf16[128,4,256]{2,1,0:T(4,128)(2,1)S(1)}, u32[]{:S(2)}, u32[]{:S(2)}) async-start(bf16[128,4,256]{2,1,0:T(4,128)(2,1)} %pad_maximum_fusion.2), calls=%async_computation.4 | async-start | bytes 524288 | tf_op jit(solution)/shard_map/all_to_all | solution.py:197
